TPU v7x, 32 devices: a whole 2x2x4 slice. The times are simulated.
32 devices in a mesh: ep: 8 (over z, y), tp: 4 (over x, core).
Axes of the slice: x: 2, y: 2, z: 4, core: 2. Of those that a mesh axis runs over, the one named last changes fastest.
Arguments:
- tokens: bfloat16 [512, 1024], P('ep', 'tp'), may hold values from -6 to 6
- conv_state: bfloat16 [512, 3, 512], P('ep', None, 'tp'), may hold values from -6 to 6
- lru_state: float32 [512, 512], P('ep', 'tp'), may hold values from -6 to 6
- mix_gain: bfloat16 [1024], replicated, may hold values from 0.099609375 to 1.8984375
- ffn_gain: bfloat16 [1024], replicated, may hold values from 0.099609375 to 1.8984375
- w_branch: bfloat16 [1024, 512], P(None, 'tp'), may hold values from -0.1875 to 0.1875
- w_gate: bfloat16 [1024, 512], P(None, 'tp'), may hold values from -0.1875 to 0.1875
- conv_taps: bfloat16 [4, 512], P(None, 'tp'), may hold values from -3 to 3
- w_recur: bfloat16 [8, 64, 64], P('tp'), may hold values from -0.75 to 0.75
- w_inject: bfloat16 [8, 64, 64], P('tp'), may hold values from -0.75 to 0.75
- lru_lambda: float32 [512], P('tp'), may hold values from 2 to 7
- w_out: bfloat16 [512, 1024], P('tp'), may hold values from -0.25 to 0.25
- expert_gate: bfloat16 [8, 1024, 2560], P('ep', None, 'tp'), may hold values from -0.1875 to 0.1875
- expert_up: bfloat16 [8, 1024, 2560], P('ep', None, 'tp'), may hold values from -0.1875 to 0.1875
- expert_down: bfloat16 [8, 2560, 1024], P('ep', 'tp'), may hold values from -0.125 to 0.125
- route_ids: int32 [512, 2], P('ep'), may hold values from 0 to 7, all different within a row; in each aligned block of 64 rows (0 to 63, 64 to 127, ...) at most 32 rows name the same one
- route_weight: float32 [512, 2], P('ep'), may hold values from 0.2 to 1
Outputs:
- mixed: bfloat16 [512, 1024], P('ep', 'tp')
- state_out: float32 [512, 512], P('ep', 'tp')
Inputs may be any that keep to these rules, and one draw needn't show every extreme that they name: `route_ids`: each row names 2 different experts. Among the 64 rows of one device no expert is named more than 32 times, and in every draw some expert is named exactly 32 times by them.
All inputs are finite; a program needn't handle non-finite values.
Results may differ from a plain program's by a relative error of at most 0.015.
Values may be sent and summed in bfloat16 or wider, within the bound.
No kernel may reach another device: no remote copies, remote signals or barrier semaphores. Data moves between devices by JAX's collectives and lax.ppermute only.
A program may use at most 64 MiB of HBM per device.

v0:
```python
import jax
import jax.numpy as jnp
from jax import lax
from jax.sharding import PartitionSpec as P

D = 1024


EPS = 1e-06
LRU_SCALE = 8.0


def rms_rows(rows, gain):
    values = rows.astype(jnp.float32)
    scaled = values * lax.rsqrt(jnp.mean(values * values, axis=-1, keepdims=True) + EPS)
    return (scaled * gain.astype(jnp.float32)).astype(jnp.bfloat16)


def body(
    tokens,
    conv_state,
    lru_state,
    mix_gain,
    ffn_gain,
    w_branch,
    w_gate,
    conv_taps,
    w_recur,
    w_inject,
    lru_lambda,
    w_out,
    expert_gate,
    expert_up,
    expert_down,
    route_ids,
    route_weight,
):
    seqs = tokens.shape[0]
    whole = lax.all_gather(tokens, "tp", axis=1, tiled=True)
    normed = rms_rows(whole, mix_gain)
    branch = jnp.dot(normed, w_branch, preferred_element_type=jnp.float32).astype(jnp.bfloat16)
    gate_in = jnp.dot(normed, w_gate, preferred_element_type=jnp.float32).astype(jnp.bfloat16)
    window = jnp.concatenate([conv_state, branch[:, None, :]], axis=1).astype(jnp.float32)
    conv_out = jnp.sum(window * conv_taps.astype(jnp.float32)[None], axis=1)
    heads_here = w_recur.shape[0]
    head_width = w_recur.shape[1]
    conv_heads = conv_out.astype(jnp.bfloat16).reshape(seqs, heads_here, head_width)
    recur = jax.nn.sigmoid(
        jnp.einsum("nhi,hij->nhj", conv_heads, w_recur, preferred_element_type=jnp.float32).reshape(
            seqs, -1
        )
    )
    inject = jax.nn.sigmoid(
        jnp.einsum(
            "nhi,hij->nhj", conv_heads, w_inject, preferred_element_type=jnp.float32
        ).reshape(seqs, -1)
    )
    log_decay = -LRU_SCALE * recur * jax.nn.softplus(-lru_lambda)
    state_out = (
        jnp.exp(log_decay) * lru_state + jnp.sqrt(-jnp.expm1(2.0 * log_decay)) * inject * conv_out
    )
    lru_out = (state_out * jax.nn.gelu(gate_in.astype(jnp.float32))).astype(jnp.bfloat16)
    partial_value = jnp.dot(lru_out, w_out, preferred_element_type=jnp.float32)
    partial_value = lax.optimization_barrier(partial_value.astype(jnp.bfloat16)).astype(jnp.float32)
    mix_out = lax.psum_scatter(
        partial_value.astype(jnp.bfloat16), "tp", scatter_dimension=1, tiled=True
    )
    resid = (tokens.astype(jnp.float32) + mix_out.astype(jnp.float32)).astype(jnp.bfloat16)
    top = route_ids.shape[1]
    local = expert_gate.shape[0]
    experts = lax.axis_size("ep") * local
    capacity = max(2, 2 * seqs * top // experts)
    flat = route_ids.reshape(-1)
    onehot = (flat[:, None] == jnp.arange(experts, dtype=jnp.int32)[None, :]).astype(jnp.int32)
    before = jnp.cumsum(onehot, axis=0) - onehot
    slot = jnp.sum(before * onehot, axis=1)
    slot_id = slot * experts + flat
    places = jnp.arange(capacity * experts, dtype=jnp.int32)
    hits = slot_id[None, :] == places[:, None]
    dispatch = jnp.sum(
        hits.reshape(capacity * experts, seqs, top).astype(jnp.float32), axis=2
    ).astype(jnp.bfloat16)
    spread = jnp.transpose(hits).reshape(seqs, top, capacity * experts)
    combine = jnp.sum(jnp.where(spread, route_weight[:, :, None], 0.0), axis=1)
    values = resid.astype(jnp.float32)
    total = lax.psum(jnp.sum(values * values, axis=1), "tp")
    quarter = values.shape[1]
    start = lax.axis_index("tp") * quarter
    gain_here = lax.dynamic_slice_in_dim(ffn_gain, start, quarter, 0).astype(jnp.float32)
    scale = lax.rsqrt(total[:, None] / D + EPS)
    normed_part = (values * scale * gain_here).astype(jnp.bfloat16)
    buffer = jnp.dot(dispatch, normed_part, preferred_element_type=jnp.float32).astype(jnp.bfloat16)
    buffer = buffer.reshape(capacity, experts, -1)
    block = lax.all_gather(
        lax.all_to_all(buffer, "ep", split_axis=1, concat_axis=1, tiled=True),
        "tp",
        axis=2,
        tiled=True,
    )
    count = block.shape[0]
    width = block.shape[2]
    grid = block.reshape(count, -1, local, width)
    rows = grid[:, :, 0].reshape(-1, width)
    first = jnp.dot(rows, expert_gate[0], preferred_element_type=jnp.float32)
    second = jnp.dot(rows, expert_up[0], preferred_element_type=jnp.float32)
    hidden = (jax.nn.silu(first) * second).astype(jnp.bfloat16)
    term = jnp.dot(hidden, expert_down[0], preferred_element_type=jnp.float32)
    term = lax.optimization_barrier(term.astype(jnp.bfloat16)).astype(jnp.float32)
    summed = lax.psum_scatter(term.astype(jnp.bfloat16), "tp", scatter_dimension=1, tiled=True)
    results = summed.reshape(count, -1, 1, summed.shape[1])
    answered = results.reshape(count, -1, results.shape[3])
    returned = lax.all_to_all(answered, "ep", split_axis=1, concat_axis=1, tiled=True)
    back = returned.reshape(capacity * experts, -1).astype(jnp.float32)
    moe = jnp.dot(combine, back, precision=lax.Precision.HIGHEST)
    mixed = (resid.astype(jnp.float32) + moe).astype(jnp.bfloat16)
    return (mixed, state_out)


def solution(mesh):
    placed = (
        P("ep", "tp"),
        P("ep", None, "tp"),
        P("ep", "tp"),
        P(),
        P(),
        P(None, "tp"),
        P(None, "tp"),
        P(None, "tp"),
        P("tp", None, None),
        P("tp", None, None),
        P("tp"),
        P("tp", None),
        P("ep", None, "tp"),
        P("ep", None, "tp"),
        P("ep", "tp", None),
        P("ep", None),
        P("ep", None),
    )
    return jax.shard_map(
        body, mesh=mesh, in_specs=placed, out_specs=(P("ep", "tp"), P("ep", "tp")), check_vma=False
    )
```

profile of v0, /device:TPU:0, one launch (start us, length us, event | category | flops | bytes accessed | tf_op | source)
XLA Modules:
  0.0 115.1 jit_solution(7022483541440773781)
XLA Ops:
  7.2 0.0 copy-start
  7.2 0.0 reduce-scatter.3.cloned.1.call-start
  7.3 6.9 %all_gather.6 = bf16[64,1024]{1,0:T(8,128)(2,1)S(1)} all-gather(bf16[64,256]{1,0:T(8,128)(2,1)} %param.17), channel_id=1, replica_groups=mesh['ep'=8,'tp'=4] {'tp'}, dimensions={1}, use_global_device_ids=true | all-gather | bytes 163840 | tf_op jit(solution)/shard_map/all_gather | solution.py:39
  14.1 0.1 fusion.38
  14.3 0.7 convert_element_type.84
  15.0 0.7 convert_element_type.88
  15.6 1.2 %fusion.28 = bf16[64,1,128]{2,0,1:T(8,128)(2,1)S(1)} fusion(bf16[1024,128]{1,0:T(8,128)(2,1)} %param.22, bf16[64,1024]{1,0:T(8,128)(2,1)S(1)} %all_gather.6, f32[1024]{0:T(1024)S(1)} %convert_element_type.84, f32[64]{0:T(128)S(1)} %add_rsqrt_fusion.1), kind=kOutput, calls=%fused_computation.27 | convolution fusion | flops 17047552 | bytes 413952 | tf_op jit(solution)/shard_map/dot_general | solution.py:41
  16.8 0.0 copy-start.8
  16.8 0.8 multiply_reduce_fusion
  17.7 0.1 convert_element_type.90
  17.8 0.9 fusion.25
  18.7 0.1 copy.64
  18.7 0.1 div.24
  18.8 0.1 fusion.21
  19.0 0.1 copy.66
  19.1 0.1 div.26
  19.2 0.0 copy-done.7
  19.2 0.0 copy-done.5
  19.2 0.0 copy-done.4
  19.3 0.0 copy-start.6
  19.3 1.0 convolution_convert_fusion
  20.3 0.0 reduce-scatter.3.cloned.1.call-update
  20.3 0.0 reduce-scatter.5.cloned.1.call-start
  20.4 0.1 copy.67
  20.5 0.1 eq.37
  20.6 0.1 fusion.46
  20.7 0.2 reduce_window_sum.11
  20.9 0.2 select_reduce_fusion.1
  21.1 0.1 mul.152
  21.2 0.1 copy.68
  21.3 0.8 dynamic-slice_convert_fusion
  22.1 0.1 convert_reduce_fusion
  22.2 19.6 %reduce-scatter.3.cloned.1.call-done = bf16[64,256]{1,0:T(8,128)(2,1)} async-done(((bf16[64,1024]{1,0:T(8,128)(2,1)}), bf16[64,256]{1,0:T(8,128)(2,1)}) %reduce-scatter.3.cloned.1.call-update) | async-done | bytes 32784 | tf_op jit(solution)/shard_map/reduce_scatter | solution.py:65
  41.8 0.9 fusion.43
  42.6 5.8 %psum.7 = f32[64]{0:T(128)S(1)} all-reduce(f32[64]{0:T(128)S(1)} %fusion.43), channel_id=1, replica_groups=mesh['ep'=8,'tp'=4] {'tp'}, use_global_device_ids=true, to_apply=%region_8.9 | all-reduce | flops 64 | bytes 512 | tf_op jit(solution)/shard_map/psum | solution.py:86
  48.4 1.0 fusion.17
  49.4 12.8 %all_to_all.10 = bf16[32,8,256]{2,0,1:T(8,128)(2,1)S(1)} all-to-all(bf16[32,8,256]{2,0,1:T(8,128)(2,1)S(1)} %copy.69), channel_id=1, replica_groups=mesh['ep'=8,'tp'=4] {'ep'}, dimensions={1} | all-to-all | bytes 262144 | tf_op jit(solution)/shard_map/all_to_all | solution.py:95
  62.2 0.1 copy.70
  62.3 6.5 %all_gather.7 = bf16[32,8,1024]{2,1,0:T(8,128)(2,1)S(1)} all-gather(bf16[32,8,256]{2,1,0:T(8,128)(2,1)S(1)} %copy.70), channel_id=1, replica_groups=mesh['ep'=8,'tp'=4] {'tp'}, dimensions={2}, use_global_device_ids=true | all-gather | bytes 655360 | tf_op jit(solution)/shard_map/all_gather | solution.py:94
  68.8 1.4 %fusion.4 = f32[256,640]{1,0:T(8,128)} fusion(bf16[1,1024,640]{2,1,0:T(8,128)(2,1)S(1)} %copy-done.1, bf16[32,8,1024]{2,1,0:T(8,128)(2,1)S(1)} %all_gather.7), kind=kOutput, calls=%fused_computation.4 | convolution fusion | flops 335544320 | bytes 2490368 | tf_op jit(solution)/shard_map/dot_general | solution.py:104
  70.3 3.3 %fusion.6 = bf16[256,1024]{1,0:T(8,128)(2,1)} fusion(bf16[1,640,1024]{2,1,0:T(8,128)(2,1)S(1)} %copy-done, bf16[1,1024,640]{2,1,0:T(8,128)(2,1)} %param.30, f32[256,640]{1,0:T(8,128)} %fusion.4, bf16[32,8,1024]{2,1,0:T(8,128)(2,1)S(1)} %all_gather.7), kind=kOutput, calls=%fused_computation.6 | convolution fusion | flops 672333824 | bytes 4325376 | tf_op jit(solution)/shard_map/dot_general | solution.py:107
  73.6 0.0 reduce-scatter.5.cloned.1.call-update
  73.6 19.3 %reduce-scatter.5.cloned.1.call-done = bf16[256,256]{1,0:T(8,128)(2,1)} async-done(((bf16[256,1024]{1,0:T(8,128)(2,1)}), bf16[256,256]{1,0:T(8,128)(2,1)}) %reduce-scatter.5.cloned.1.call-update) | async-done | bytes 131088 | tf_op jit(solution)/shard_map/reduce_scatter | solution.py:109
  92.9 1.6 %copy.71 = bf16[32,8,256]{2,0,1:T(8,128)(2,1)} copy(bf16[32,8,256]{2,1,0:T(8,128)(2,1)} %bitcast.42) | data formatting | bytes 262144 | tf_op jit(solution)/shard_map/reshape;reshape | solution.py:111
  94.5 5.5 %all-to-all-start.1 = ((bf16[32,8,256]{2,0,1:T(8,128)(2,1)}), bf16[32,8,256]{2,0,1:T(8,128)(2,1)S(1)}, u32[]{:S(2)}, u32[]{:S(2)}) async-start(bf16[32,8,256]{2,0,1:T(8,128)(2,1)} %copy.71), calls=%async_computation.3 | async-start | bytes 262144 | tf_op jit(solution)/shard_map/all_to_all | solution.py:112
  100.0 0.1 select_reduce_fusion
  100.1 7.2 %all-to-all-done.1 = bf16[32,8,256]{2,0,1:T(8,128)(2,1)S(1)} async-done(((bf16[32,8,256]{2,0,1:T(8,128)(2,1)}), bf16[32,8,256]{2,0,1:T(8,128)(2,1)S(1)}, u32[]{:S(2)}, u32[]{:S(2)}) %all-to-all-start.1) | async-done | bytes 131104 | tf_op jit(solution)/shard_map/all_to_all | solution.py:112
  107.4 0.9 fusion.26
  (26 shorter events, 0.1 us)
Async XLA Ops:
  7.2 63.1 %copy-start = (bf16[1,640,1024]{2,1,0:T(8,128)(2,1)S(1)}, bf16[1,640,1024]{2,1,0:T(8,128)(2,1)}, u32[]{:S(2)}) copy-start(bf16[1,640,1024]{2,1,0:T(8,128)(2,1)} %param.31) | copy-start | bytes 3932164
  7.2 11.7 %copy-start.10 = (bf16[2,64,64]{2,1,0:T(8,128)(2,1)S(1)}, bf16[2,64,64]{2,1,0:T(8,128)(2,1)}, u32[]{:S(2)}) copy-start(bf16[2,64,64]{2,1,0:T(8,128)(2,1)} %param.26) | copy-start | bytes 49156
  7.2 12.0 %copy-start.11 = (f32[128]{0:T(128)S(1)}, f32[128]{0:T(128)}, u32[]{:S(2)}) copy-start(f32[128]{0:T(128)} %param.27) | copy-start | bytes 1540
  7.2 12.0 %copy-start.7 = (f32[64,128]{1,0:T(8,128)S(1)}, f32[64,128]{1,0:T(8,128)}, u32[]{:S(2)}) copy-start(f32[64,128]{1,0:T(8,128)} %param.19) | copy-start | bytes 98308
  7.2 12.0 %copy-start.5 = (bf16[1024,128]{1,0:T(8,128)(2,1)S(1)}, bf16[1024,128]{1,0:T(8,128)(2,1)}, u32[]{:S(2)}) copy-start(bf16[1024,128]{1,0:T(8,128)(2,1)} %param.23) | copy-start | bytes 786436
  7.2 12.0 %copy-start.4 = (bf16[128,1024]{1,0:T(8,128)(2,1)S(1)}, bf16[128,1024]{1,0:T(8,128)(2,1)}, u32[]{:S(2)}) copy-start(bf16[128,1024]{1,0:T(8,128)(2,1)} %param.28) | copy-start | bytes 786436
  7.2 34.5 %reduce-scatter.3.cloned.1.call-start = ((), (), s32[]{:S(2)}) async-start(), calls=%async_computation.4 | async-start | bytes 163840 | tf_op jit(solution)/shard_map/reduce_scatter | solution.py:65
  16.8 3.6 %copy-start.8 = (s32[64,2]{0,1:T(2,128)S(1)}, s32[64,2]{0,1:T(2,128)}, u32[]{:S(2)}) copy-start(s32[64,2]{0,1:T(2,128)} %param.32) | copy-start | bytes 1540
  17.8 24.0 %copy-start.2 = (bf16[64,256]{1,0:T(8,128)(2,1)S(1)}, bf16[64,256]{1,0:T(8,128)(2,1)}, u32[]{:S(2)}) copy-start(bf16[64,256]{1,0:T(8,128)(2,1)} %param.17) | copy-start | bytes 98308
  19.3 49.6 %copy-start.6 = (f32[64,128]{1,0:T(8,128)}, f32[64,128]{1,0:T(8,128)S(1)}, u32[]{:S(2)}) copy-start(f32[64,128]{1,0:T(8,128)S(1)} %multiply_add_fusion) | copy-start | bytes 98308
  20.3 48.5 %copy-start.1 = (bf16[1,1024,640]{2,1,0:T(8,128)(2,1)S(1)}, bf16[1,1024,640]{2,1,0:T(8,128)(2,1)}, u32[]{:S(2)}) copy-start(bf16[1,1024,640]{2,1,0:T(8,128)(2,1)} %param.29) | copy-start | bytes 3932164
  20.3 72.6 %reduce-scatter.5.cloned.1.call-start = ((), (), s32[]{:S(2)}) async-start(), calls=%async_computation.5 | async-start | bytes 655360 | tf_op jit(solution)/shard_map/reduce_scatter | solution.py:109
  70.3 29.8 %copy-start.9 = (f32[64,2]{0,1:T(2,128)S(1)}, f32[64,2]{0,1:T(2,128)}, u32[]{:S(2)}) copy-start(f32[64,2]{0,1:T(2,128)} %param.33) | copy-start | bytes 1540
  70.3 37.1 %copy-start.3 = (bf16[64,256]{1,0:T(8,128)(2,1)S(1)}, bf16[64,256]{1,0:T(8,128)(2,1)}, u32[]{:S(2)}) copy-start(bf16[64,256]{1,0:T(8,128)(2,1)} %reduce-scatter.3.cloned.1.call-done) | copy-start | bytes 98308
  94.5 12.9 %all-to-all-start.1 = ((bf16[32,8,256]{2,0,1:T(8,128)(2,1)}), bf16[32,8,256]{2,0,1:T(8,128)(2,1)S(1)}, u32[]{:S(2)}, u32[]{:S(2)}) async-start(bf16[32,8,256]{2,0,1:T(8,128)(2,1)} %copy.71), calls=%async_computation.3 | async-start | bytes 262144 | tf_op jit(solution)/shard_map/all_to_all | solution.py:112
Sparse Core Ops, SparseCore 0:
  20.4 21.2 reduce-scatter.2
  73.8 19.1 reduce-scatter.4
where the time goes:
time: 116 us; the launch traced here: 115 us
  waiting for transfers between devices  46.1 us (40%)
  blocking collectives  31.9 us (28%)
  between operations  14.3 us (12%)
  matrix products  9.9 us (9%)
  starting transfers between devices  5.6 us (5%)
  other arithmetic  4.66 us (4%)
  local copies, waits for them, and re-layouts  2.57 us (2%)
    reduce_scatter x1, waiting for transfers between devices, body(): lax.psum_scatter(partial_value.astype(jnp.bfloat16), 'tp', scatter_dimens...  19.6 us
    reduce_scatter x1, waiting for transfers between devices, body(): lax.psum_scatter(term.astype(jnp.bfloat16), 'tp', scatter_dimension=1, ti...  19.3 us
    all_to_all x1, blocking collectives, body(): lax.all_to_all(buffer, 'ep', split_axis=1, concat_axis=1, tiled=True)  12.8 us
    all_to_all x1, waiting for transfers between devices, body(): lax.all_to_all(answered, 'ep', split_axis=1, concat_axis=1, tiled=True)  7.23 us
    all_gather x1, blocking collectives, body(): whole = lax.all_gather(tokens, 'tp', axis=1, tiled=True)  6.85 us
    all_gather x1, blocking collectives, body(): lax.all_gather(lax.all_to_all(buffer, 'ep', split_axis=1, concat_axis=1,...  6.5 us
    psum x1, blocking collectives, body(): total = lax.psum(jnp.sum(values * values, axis=1), 'tp')  5.76 us
    all_to_all x1, starting transfers between devices, body(): lax.all_to_all(answered, 'ep', split_axis=1, concat_axis=1, tiled=True)  5.52 us
  transfers between devices with their start and end apart: 3, of which 3 were waited for; matrix products, arithmetic and copies ran while one was open for 2% of the time, Pallas kernels for 0%

commit v1 on v0

v1 whole, which is shorter than its diff:
```python
import jax
import jax.numpy as jnp
import numpy as np
from jax import lax
from jax.sharding import Mesh, PartitionSpec as P

EPS = 1e-06
LRU_SCALE = 8.0
SWAP = ((0, 1), (1, 0))


def rms_rows(rows, gain):
    values = rows.astype(jnp.float32)
    scaled = values * lax.rsqrt(jnp.mean(values * values, axis=-1, keepdims=True) + EPS)
    return (scaled * gain.astype(jnp.float32)).astype(jnp.bfloat16)


def body(
    tokens,
    conv_state,
    lru_state,
    mix_gain,
    ffn_gain,
    w_branch,
    w_gate,
    conv_taps,
    w_recur,
    w_inject,
    lru_lambda,
    w_out,
    expert_gate,
    expert_up,
    expert_down,
    route_ids,
    route_weight,
):
    seqs, quarter = tokens.shape
    n_ep = lax.axis_size("ep")
    tp = ("xa", "xb")
    na, nb = lax.axis_size("xa"), lax.axis_size("xb")
    n_tp = na * nb
    me = lax.axis_index(tp)
    others = [
        lax.ppermute(tokens, tp, [(i, i ^ k) for i in range(n_tp)]) for k in range(1, n_tp)
    ]
    pieces = jnp.stack([tokens] + others)
    whole = jnp.concatenate(
        [lax.dynamic_index_in_dim(pieces, me ^ t, 0, keepdims=False) for t in range(n_tp)], axis=1
    )
    normed = rms_rows(whole, mix_gain)
    branch = jnp.dot(normed, w_branch, preferred_element_type=jnp.float32).astype(jnp.bfloat16)
    gate_in = jnp.dot(normed, w_gate, preferred_element_type=jnp.float32).astype(jnp.bfloat16)
    window = jnp.concatenate([conv_state, branch[:, None, :]], axis=1).astype(jnp.float32)
    conv_out = jnp.sum(window * conv_taps.astype(jnp.float32)[None], axis=1)
    heads_here = w_recur.shape[0]
    head_width = w_recur.shape[1]
    conv_heads = conv_out.astype(jnp.bfloat16).reshape(seqs, heads_here, head_width)
    recur = jax.nn.sigmoid(
        jnp.einsum("nhi,hij->nhj", conv_heads, w_recur, preferred_element_type=jnp.float32).reshape(
            seqs, -1
        )
    )
    inject = jax.nn.sigmoid(
        jnp.einsum(
            "nhi,hij->nhj", conv_heads, w_inject, preferred_element_type=jnp.float32
        ).reshape(seqs, -1)
    )
    log_decay = -LRU_SCALE * recur * jax.nn.softplus(-lru_lambda)
    state_out = (
        jnp.exp(log_decay) * lru_state + jnp.sqrt(-jnp.expm1(2.0 * log_decay)) * inject * conv_out
    )
    lru_out = (state_out * jax.nn.gelu(gate_in.astype(jnp.float32))).astype(jnp.bfloat16)
    partial_value = jnp.dot(lru_out, w_out, preferred_element_type=jnp.float32).astype(jnp.bfloat16)
    split = partial_value.reshape(seqs, n_tp, quarter)
    mix_out = lax.dynamic_index_in_dim(split, me, 1, keepdims=False).astype(jnp.float32)
    for k in range(1, n_tp):
        out = lax.dynamic_index_in_dim(split, me ^ k, 1, keepdims=False)
        mix_out = mix_out + lax.ppermute(
            out, tp, [(i, i ^ k) for i in range(n_tp)]
        ).astype(jnp.float32)
    resid = (tokens.astype(jnp.float32) + mix_out.astype(jnp.bfloat16).astype(jnp.float32)).astype(
        jnp.bfloat16
    )
    top = route_ids.shape[1]
    local = expert_gate.shape[0]
    experts = n_ep * local
    capacity = max(2, 2 * seqs * top // experts)
    slots = experts * capacity
    flat = route_ids.reshape(-1)
    onehot = (flat[:, None] == jnp.arange(experts, dtype=jnp.int32)[None, :]).astype(jnp.int32)
    before = jnp.cumsum(onehot, axis=0) - onehot
    slot = jnp.sum(before * onehot, axis=1)
    slot_id = flat * capacity + slot
    hits = (slot_id.reshape(seqs, top)[:, :, None] == jnp.arange(slots, dtype=jnp.int32)).astype(
        jnp.bfloat16
    )
    dispatch = jnp.sum(hits, axis=1)
    buffer = lax.dot_general(
        dispatch, resid, (((0,), (0,)), ((), ())), preferred_element_type=jnp.float32
    ).astype(jnp.bfloat16)
    sent = jnp.broadcast_to(buffer[None], (na, slots, quarter)).reshape(na * slots, quarter)
    mine = lax.all_to_all(sent, ("xa", "ep"), split_axis=0, concat_axis=0, tiled=True)
    theirs = lax.ppermute(mine, "xb", SWAP)
    b = lax.axis_index("xb")
    first_b = jnp.where(b == 0, mine, theirs).reshape(na, slots, quarter)
    second_b = jnp.where(b == 0, theirs, mine).reshape(na, slots, quarter)
    rows = jnp.stack([first_b, second_b], axis=1).transpose(2, 0, 1, 3).reshape(slots, -1)
    rows = rms_rows(rows, ffn_gain)
    first = jnp.dot(rows, expert_gate[0], preferred_element_type=jnp.float32)
    second = jnp.dot(rows, expert_up[0], preferred_element_type=jnp.float32)
    hidden = (jax.nn.silu(first) * second).astype(jnp.bfloat16)
    term = jnp.dot(hidden, expert_down[0], preferred_element_type=jnp.float32).astype(jnp.bfloat16)
    term = term.reshape(slots, na, nb, quarter).transpose(2, 1, 0, 3).reshape(nb, na * slots, quarter)
    keep = lax.dynamic_index_in_dim(term, b, 0, keepdims=False)
    give = lax.dynamic_index_in_dim(term, 1 - b, 0, keepdims=False)
    pair = (
        keep.astype(jnp.float32) + lax.ppermute(give, "xb", SWAP).astype(jnp.float32)
    ).astype(jnp.bfloat16)
    back = lax.all_to_all(pair, ("xa", "ep"), split_axis=0, concat_axis=0, tiled=True)
    back = back.reshape(na, slots, quarter)
    moe = jnp.zeros((seqs, quarter), jnp.float32)
    for k in range(top):
        picked = sum(
            jnp.dot(hits[:, k], back[a], preferred_element_type=jnp.float32) for a in range(na)
        )
        moe = moe + picked * route_weight[:, k, None]
    mixed = (resid.astype(jnp.float32) + moe).astype(jnp.bfloat16)
    return (mixed, state_out)


def solution(mesh):
    n_ep, n_tp = mesh.shape["ep"], mesh.shape["tp"]
    finer = Mesh(np.asarray(mesh.devices).reshape(n_ep, n_tp // 2, 2), ("ep", "xa", "xb"))
    tp = ("xa", "xb")
    placed = (
        P("ep", tp),
        P("ep", None, tp),
        P("ep", tp),
        P(),
        P(),
        P(None, tp),
        P(None, tp),
        P(None, tp),
        P(tp, None, None),
        P(tp, None, None),
        P(tp),
        P(tp, None),
        P("ep", None, tp),
        P("ep", None, tp),
        P("ep", tp, None),
        P("ep", None),
        P("ep", None),
    )
    return jax.shard_map(
        body, mesh=finer, in_specs=placed, out_specs=(P("ep", tp), P("ep", tp)), check_vma=False
    )
```

time: 116 us -> 59.2 us (0.51)
  waiting for transfers between devices: 46.1 us -> 16.7 us
  blocking collectives: 31.9 us -> 16 us
  between operations: 14.3 us -> 1.03 us
  starting transfers between devices: 5.6 us -> 9.06 us
  matrix products: 9.9 us -> 7.68 us
    reduce_scatter x2 -> x0, waiting for transfers between devices: 38.9 us -> none  [the longest x1 19.6 us: body(): lax.psum_scatter(partial_value.astype(jnp.bfloat16), 'tp', scatter_dimens...]
    all_gather x2 -> x0, blocking collectives: 13.4 us -> none  [the longest x1 6.85 us: body(): whole = lax.all_gather(tokens, 'tp', axis=1, tiled=True)]
    ppermute x0 -> x8, waiting for transfers between devices: none -> 6.45 us  [the longest x3 3.53 us: body(): lax.ppermute(out, tp, [(i, i ^ k) for i in range(n_tp)]).astype(jnp.float32)]
    psum x1 -> x0, blocking collectives: 5.76 us -> none  [body(): total = lax.psum(jnp.sum(values * values, axis=1), 'tp')]
    ppermute x0 -> x8, starting transfers between devices: none -> 5.53 us  [the longest x3 3.15 us: body(): lax.ppermute(tokens, tp, [(i, i ^ k) for i in range(n_tp)])]
    all_to_all x1, blocking collectives: 12.8 us -> 16 us  [body(): lax.all_to_all(sent, ('xa', 'ep'), split_axis=0, concat_axis=0, tiled=True)]
    all_to_all x1, waiting for transfers between devices: 7.23 us -> 10.3 us  [body(): lax.all_to_all(pair, ('xa', 'ep'), split_axis=0, concat_axis=0, tiled=True)]
    all_to_all x1, starting transfers between devices: 5.52 us -> 3.53 us  [body(): lax.all_to_all(pair, ('xa', 'ep'), split_axis=0, concat_axis=0, tiled=True)]
  transfers between devices with their start and end apart: 3 -> 9, of which waited for: 3 -> 5; matrix products, arithmetic and copies ran while one was open for 2% -> 8% of each run, Pallas kernels for 0% -> 0%
where the time goes in v1:
time: 59.2 us; the launch traced here: 58.7 us
  waiting for transfers between devices  16.7 us (28%)
  blocking collectives  16 us (27%)
  starting transfers between devices  9.06 us (15%)
  matrix products  7.68 us (13%)
  other arithmetic  5.54 us (9%)
  local copies, waits for them, and re-layouts  2.7 us (5%)
  between operations  1.03 us (2%)
    all_to_all x1, blocking collectives, body(): lax.all_to_all(sent, ('xa', 'ep'), split_axis=0, concat_axis=0, tiled=True)  16 us
    all_to_all x1, waiting for transfers between devices, body(): lax.all_to_all(pair, ('xa', 'ep'), split_axis=0, concat_axis=0, tiled=True)  10.3 us
    ppermute x3, waiting for transfers between devices, body(): lax.ppermute(out, tp, [(i, i ^ k) for i in range(n_tp)]).astype(jnp.float32)  3.53 us
    all_to_all x1, starting transfers between devices, body(): lax.all_to_all(pair, ('xa', 'ep'), split_axis=0, concat_axis=0, tiled=True)  3.53 us
    ppermute x3, starting transfers between devices, body(): lax.ppermute(tokens, tp, [(i, i ^ k) for i in range(n_tp)])  3.15 us
    dot_general x1, matrix products, body(): jnp.dot(hidden, expert_down[0], preferred_element_type=jnp.float32)  2.44 us
    ppermute x3, starting transfers between devices, body(): lax.ppermute(out, tp, [(i, i ^ k) for i in range(n_tp)]).astype(jnp.float32)  2.17 us
    dot_general x1, matrix products, body(): first = jnp.dot(rows, expert_gate[0], preferred_element_type=jnp.float32)  1.92 us
  transfers between devices with their start and end apart: 9, of which 5 were waited for; matrix products, arithmetic and copies ran while one was open for 8% of the time, Pallas kernels for 0%

profile of v1, /device:TPU:0, one launch (start us, length us, event | category | flops | bytes accessed | tf_op | source)
XLA Modules:
  0.0 58.7 jit_solution(8125251669470570432)
XLA Ops:
  0.7 0.6 collective-permute-start
  1.2 2.6 %collective-permute-start.1 = (bf16[64,256]{1,0:T(8,128)(2,1)}, bf16[64,256]{1,0:T(8,128)(2,1)S(1)}, u32[]{:S(2)}, u32[]{:S(2)}) collective-permute-start(bf16[64,256]{1,0:T(8,128)(2,1)} %param.17), channel_id=1, source_target_pairs={{0,2},{1,3},{2,0},{3,1},{4,6},{5,7},{6,4},{7,5},{8,10},{9,11},{10,... | collective-permute-start | bytes 98312 | tf_op jit(solution)/shard_map/ppermute | solution.py:44
  3.8 0.8 %copy.61 = s32[64,2]{1,0:T(8,128)S(1)} copy(s32[64,2]{0,1:T(2,128)} %param.32) | data formatting | bytes 1024 | tf_op args[15]
  4.6 0.1 eq.32
  4.7 0.1 fusion.49
  4.8 0.2 reduce_window_sum.11
  5.0 0.2 select_reduce_fusion
  5.2 0.1 reduce_sum.53
  5.4 0.7 %multiply_add_fusion.1 = s32[64,2]{0,1:T(2,128)S(1)} fusion(s32[64,2]{0,1:T(2,128)S(1)} %copy.62, s32[64,2]{0,1:T(2,128)} %param.32), kind=kLoop, calls=%fused_computation.103 | loop fusion | flops 256 | bytes 1536 | tf_op jit(solution)/shard_map/add | solution.py:93
  6.1 0.7 %fusion.77 = f32[128]{0:T(128)S(1)} fusion(f32[128]{0:T(128)} %param.27), kind=kLoop, calls=%fused_computation.104 | loop fusion | flops 1024 | bytes 1024 | tf_op jit(solution)/shard_map/mul | solution.py:68
  6.8 0.7 %convert_element_type.119 = f32[1024]{0:T(1024)S(1)} convert(bf16[1024]{0:T(1024)(128)(2,1)} %param.20) | non-fusion elementwise | flops 1024 | bytes 6144 | tf_op jit(solution)/shard_map/convert_element_type | solution.py:15
  7.4 0.7 %convert_element_type.123 = f32[4,128]{1,0:T(4,128)S(1)} convert(bf16[4,128]{1,0:T(4,128)(2,1)} %param.24) | non-fusion elementwise | flops 512 | bytes 3072 | tf_op jit(solution)/shard_map/convert_element_type | solution.py:54
  8.1 0.8 %pad_maximum_fusion.1 = bf16[4,64,256]{2,1,0:T(8,128)(2,1)S(1)} fusion(bf16[1,64,256]{2,1,0:T(8,128)(2,1)S(1)} %bitcast.114, bf16[1,64,256]{2,1,0:T(8,128)(2,1)S(1)} %bitcast.113, bf16[1,64,256]{2,1,0:T(8,128)(2,1)S(1)} %bitcast.112, bf16[1,64,256]{2,1,0:T(8,128)(2,1)} %bitcast.108), kind=kLoop, calls=%fused_computation.55 | loop fusion | flops 196608 | bytes 262144 | tf_op jit(solution)/shard_map/stack | solution.py:46
  9.0 0.1 fusion.43
  9.1 1.2 %fusion.31 = bf16[64,1,128]{2,0,1:T(8,128)(2,1)S(1)} fusion(bf16[1024,128]{1,0:T(8,128)(2,1)} %param.22, f32[1024]{0:T(1024)S(1)} %convert_element_type.119, f32[64]{0:T(128)S(1)} %add_rsqrt_fusion.1, bf16[64,256]{1,0:T(8,128)(2,1)S(1)} %get-tuple-element.11, bf16[64,256]{1,0:T(8,128)(2,1)S(1)} %get-tuple-element.12, ...), kind=kOutput, calls=%fused_computation.33 | convolution fusion | flops 17506304 | bytes 413952 | tf_op jit(solution)/shard_map/dot_general | solution.py:51
  10.4 0.1 convert_element_type.125
  10.5 0.1 fusion.27
  10.7 0.1 div.31
  10.8 0.1 fusion.23
  11.0 0.1 div.33
  11.2 0.4 convolution_convert_fusion
  11.6 0.1 reshape.99
  11.7 0.3 constant_dynamic-slice_fusion.3
  12.0 0.2 collective-permute-start.3
  12.2 1.9 %collective-permute-start.4 = (bf16[64,256]{1,0:T(8,128)(2,1)S(1)}, bf16[64,256]{1,0:T(8,128)(2,1)S(1)}, u32[]{:S(2)}, u32[]{:S(2)}) collective-permute-start(bf16[64,256]{1,0:T(8,128)(2,1)S(1)} %bitcast.110), channel_id=1, source_target_pairs={{0,2},{1,3},{2,0},{3,1},{4,6},{5,7},{6,4},{7,5},{8,10},{9,11},{10,... | collective-permute-start | bytes 98312 | tf_op jit(solution)/shard_map/ppermute | solution.py:78
  14.2 0.1 convert_reduce_fusion
  14.3 1.9 %collective-permute-done.4 = bf16[64,256]{1,0:T(8,128)(2,1)S(1)} collective-permute-done((bf16[64,256]{1,0:T(8,128)(2,1)S(1)}, bf16[64,256]{1,0:T(8,128)(2,1)S(1)}, u32[]{:S(2)}, u32[]{:S(2)}) %collective-permute-start.4) | collective-permute-done | bytes 32800 | tf_op jit(solution)/shard_map/ppermute | solution.py:78
  16.1 1.7 %collective-permute-done.5 = bf16[64,256]{1,0:T(8,128)(2,1)S(1)} collective-permute-done((bf16[64,256]{1,0:T(8,128)(2,1)S(1)}, bf16[64,256]{1,0:T(8,128)(2,1)S(1)}, u32[]{:S(2)}, u32[]{:S(2)}) %collective-permute-start.5) | collective-permute-done | bytes 32800 | tf_op jit(solution)/shard_map/ppermute | solution.py:78
  17.8 0.2 convolution_convert_fusion.1
  18.1 16.0 %all_to_all.21 = bf16[16,32,256]{2,1,0:T(8,128)(2,1)S(1)} all-to-all(bf16[16,32,256]{2,1,0:T(8,128)(2,1)S(1)} %bitcast.106), channel_id=1, replica_groups=mesh['ep'=8,'xa'=2,'xb'=2] {'xa','ep'}, dimensions={0} | all-to-all | bytes 524288 | tf_op jit(solution)/shard_map/all_to_all | solution.py:102
  34.1 1.5 %collective-permute-done.6 = bf16[512,256]{1,0:T(8,128)(2,1)S(1)} collective-permute-done((bf16[512,256]{1,0:T(8,128)(2,1)S(1)}, bf16[512,256]{1,0:T(8,128)(2,1)S(1)}, u32[]{:S(2)}, u32[]{:S(2)}) %collective-permute-start.6) | collective-permute-done | bytes 262176 | tf_op jit(solution)/shard_map/ppermute | solution.py:103
  35.6 0.2 fusion.32
  35.8 0.2 fusion.40
  36.0 0.2 copy.64
  36.2 1.9 %fusion.4 = f32[256,640]{1,0:T(8,128)S(1)} fusion(bf16[256,1024]{0,1:T(8,128)(2,1)S(1)} %bitcast.98, bf16[1,1024,640]{2,1,0:T(8,128)(2,1)} %param.29), kind=kOutput, calls=%fused_computation.6 | convolution fusion | flops 335544320 | bytes 2490368 | tf_op jit(solution)/shard_map/dot_general | solution.py:109
  38.2 2.4 %fusion.6 = bf16[256,1024]{1,0:T(8,128)(2,1)S(1)} fusion(bf16[1,640,1024]{2,1,0:T(8,128)(2,1)S(1)} %copy-done, bf16[256,1024]{0,1:T(8,128)(2,1)S(1)} %bitcast.99, bf16[1,1024,640]{2,1,0:T(8,128)(2,1)} %param.30, f32[256,640]{1,0:T(8,128)S(1)} %fusion.4), kind=kOutput, calls=%fused_computation.8 | convolution fusion | flops 672333824 | bytes 4325376 | tf_op jit(solution)/shard_map/dot_general | solution.py:112
  40.6 0.4 reshape.100
  41.0 0.1 copy.65
  41.1 0.2 collective-permute-start.7
  41.3 1.4 %collective-permute-done.7 = bf16[512,256]{1,0:T(8,128)(2,1)S(1)} collective-permute-done((bf16[512,256]{1,0:T(8,128)(2,1)S(1)}, bf16[512,256]{1,0:T(8,128)(2,1)S(1)}, u32[]{:S(2)}, u32[]{:S(2)}) %collective-permute-start.7) | collective-permute-done | bytes 262176 | tf_op jit(solution)/shard_map/ppermute | solution.py:117
  42.7 0.8 %fusion.41 = bf16[512,256]{1,0:T(8,128)(2,1)} fusion(bf16[512,256]{1,0:T(8,128)(2,1)S(1)} %collective-permute-done.7, bf16[2,512,256]{2,1,0:T(8,128)(2,1)S(1)} %bitcast.101, s32[]{:T(128)S(6)} %select_n.49), kind=kLoop, calls=%fused_computation.45 | loop fusion | flops 524288 | bytes 786436 | tf_op jit(solution)/shard_map/convert_element_type | solution.py:118
  43.5 3.5 %all-to-all-start.1 = ((bf16[16,32,256]{2,1,0:T(8,128)(2,1)}), bf16[16,32,256]{2,1,0:T(8,128)(2,1)S(1)}, u32[]{:S(2)}, u32[]{:S(2)}) async-start(bf16[16,32,256]{2,1,0:T(8,128)(2,1)} %bitcast.30), calls=%async_computation.1 | async-start | bytes 524288 | tf_op jit(solution)/shard_map/all_to_all | solution.py:119
  47.1 0.1 iota_compare_fusion
  47.1 10.3 %all-to-all-done.1 = bf16[16,32,256]{2,1,0:T(8,128)(2,1)S(1)} async-done(((bf16[16,32,256]{2,1,0:T(8,128)(2,1)}), bf16[16,32,256]{2,1,0:T(8,128)(2,1)S(1)}, u32[]{:S(2)}, u32[]{:S(2)}) %all-to-all-start.1) | async-done | bytes 262176 | tf_op jit(solution)/shard_map/all_to_all | solution.py:119
  57.5 0.1 fusion.51
  57.6 0.2 fusion.50
  57.8 0.2 fusion.19
  57.9 0.8 %fusion.29 = bf16[64,256]{1,0:T(8,128)(2,1)} fusion(f32[64,256]{1,0:T(8,128)S(1)} %fusion.19, f32[64,256]{1,0:T(8,128)S(1)} %fusion.51, bf16[256,256]{1,0:T(8,128)(2,1)S(1)} %bitcast.103, bf16[64,256]{1,0:T(8,128)(2,1)S(1)} %add_convert_fusion, pred[64,2,256]{2,0,1:T(32,128)(4,1)S(1)} %iota_compare_fusion, f32[64]{0:T(128)S(1)} %get-tuple-element.14), kind=kOutput, calls=%fused_computation.29 | convolution fusion | flops 8486912 | bytes 344576 | tf_op jit(solution)/shard_map/dot_general | solution.py:124
  (49 shorter events, 0.6 us)
Async XLA Ops:
  0.6 37.5 %copy-start = (bf16[1,640,1024]{2,1,0:T(8,128)(2,1)S(1)}, bf16[1,640,1024]{2,1,0:T(8,128)(2,1)}, u32[]{:S(2)}) copy-start(bf16[1,640,1024]{2,1,0:T(8,128)(2,1)} %param.31) | copy-start | bytes 3932164
  0.6 9.7 %copy-start.2 = (bf16[64,3,128]{2,0,1:T(8,128)(2,1)S(1)}, bf16[64,3,128]{2,0,1:T(8,128)(2,1)}, u32[]{:S(2)}) copy-start(bf16[64,3,128]{2,0,1:T(8,128)(2,1)} %param.18) | copy-start | bytes 147460
  0.7 9.8 %copy-start.9 = (bf16[2,64,64]{2,1,0:T(8,128)(2,1)S(1)}, bf16[2,64,64]{2,1,0:T(8,128)(2,1)}, u32[]{:S(2)}) copy-start(bf16[2,64,64]{2,1,0:T(8,128)(2,1)} %param.25) | copy-start | bytes 49156
  0.7 7.5 %collective-permute-start = (bf16[64,256]{1,0:T(8,128)(2,1)}, bf16[64,256]{1,0:T(8,128)(2,1)S(1)}, u32[]{:S(2)}, u32[]{:S(2)}) collective-permute-start(bf16[64,256]{1,0:T(8,128)(2,1)} %param.17), channel_id=1, source_target_pairs={{0,1},{1,0},{2,3},{3,2},{4,5},{5,4},{6,7},{7,6},{8,9},{9,8},{10,11... | collective-permute-start | bytes 98312 | tf_op jit(solution)/shard_map/ppermute | solution.py:44
  1.2 6.9 %collective-permute-start.1 = (bf16[64,256]{1,0:T(8,128)(2,1)}, bf16[64,256]{1,0:T(8,128)(2,1)S(1)}, u32[]{:S(2)}, u32[]{:S(2)}) collective-permute-start(bf16[64,256]{1,0:T(8,128)(2,1)} %param.17), channel_id=1, source_target_pairs={{0,2},{1,3},{2,0},{3,1},{4,6},{5,7},{6,4},{7,5},{8,10},{9,11},{10,... | collective-permute-start | bytes 98312 | tf_op jit(solution)/shard_map/ppermute | solution.py:44
  3.8 4.4 %collective-permute-start.2 = (bf16[64,256]{1,0:T(8,128)(2,1)}, bf16[64,256]{1,0:T(8,128)(2,1)S(1)}, u32[]{:S(2)}, u32[]{:S(2)}) collective-permute-start(bf16[64,256]{1,0:T(8,128)(2,1)} %param.17), channel_id=1, source_target_pairs={{0,3},{1,2},{2,1},{3,0},{4,7},{5,6},{6,5},{7,4},{8,11},{9,10},{10,... | collective-permute-start | bytes 98312 | tf_op jit(solution)/shard_map/ppermute | solution.py:44
  4.6 6.2 %copy-start.10 = (bf16[2,64,64]{2,1,0:T(8,128)(2,1)S(1)}, bf16[2,64,64]{2,1,0:T(8,128)(2,1)}, u32[]{:S(2)}) copy-start(bf16[2,64,64]{2,1,0:T(8,128)(2,1)} %param.26) | copy-start | bytes 49156
  8.9 2.2 %copy-start.3 = (f32[64,128]{1,0:T(8,128)S(1)}, f32[64,128]{1,0:T(8,128)}, u32[]{:S(2)}) copy-start(f32[64,128]{1,0:T(8,128)} %param.19) | copy-start | bytes 98308
  8.9 2.2 %copy-start.7 = (bf16[128,1024]{1,0:T(8,128)(2,1)S(1)}, bf16[128,1024]{1,0:T(8,128)(2,1)}, u32[]{:S(2)}) copy-start(bf16[128,1024]{1,0:T(8,128)(2,1)} %param.28) | copy-start | bytes 786436
  8.9 2.2 %copy-start.8 = (bf16[1024,128]{1,0:T(8,128)(2,1)S(1)}, bf16[1024,128]{1,0:T(8,128)(2,1)}, u32[]{:S(2)}) copy-start(bf16[1024,128]{1,0:T(8,128)(2,1)} %param.23) | copy-start | bytes 786436
  10.9 6.9 %copy-start.1 = (bf16[64,256]{1,0:T(8,128)(2,1)S(1)}, bf16[64,256]{1,0:T(8,128)(2,1)}, u32[]{:S(2)}) copy-start(bf16[64,256]{1,0:T(8,128)(2,1)} %param.17) | copy-start | bytes 98308
  11.2 6.9 %copy-start.4 = (f32[64,128]{1,0:T(8,128)}, f32[64,128]{1,0:T(8,128)S(1)}, u32[]{:S(2)}) copy-start(f32[64,128]{1,0:T(8,128)S(1)} %multiply_add_fusion) | copy-start | bytes 98308
  11.6 22.5 %copy-start.5 = (bf16[1024]{0:T(1024)(128)(2,1)S(1)}, bf16[1024]{0:T(1024)(128)(2,1)}, u32[]{:S(2)}) copy-start(bf16[1024]{0:T(1024)(128)(2,1)} %param.21) | copy-start | bytes 6148
  12.0 2.3 %collective-permute-start.3 = (bf16[64,256]{1,0:T(8,128)(2,1)S(1)}, bf16[64,256]{1,0:T(8,128)(2,1)S(1)}, u32[]{:S(2)}, u32[]{:S(2)}) collective-permute-start(bf16[64,256]{1,0:T(8,128)(2,1)S(1)} %bitcast.109), channel_id=1, source_target_pairs={{0,1},{1,0},{2,3},{3,2},{4,5},{5,4},{6,7},{7,6},{8,9},{9,8},{10,11... | collective-permute-start | bytes 98312 | tf_op jit(solution)/shard_map/ppermute | solution.py:78
  12.2 3.9 %collective-permute-start.4 = (bf16[64,256]{1,0:T(8,128)(2,1)S(1)}, bf16[64,256]{1,0:T(8,128)(2,1)S(1)}, u32[]{:S(2)}, u32[]{:S(2)}) collective-permute-start(bf16[64,256]{1,0:T(8,128)(2,1)S(1)} %bitcast.110), channel_id=1, source_target_pairs={{0,2},{1,3},{2,0},{3,1},{4,6},{5,7},{6,4},{7,5},{8,10},{9,11},{10,... | collective-permute-start | bytes 98312 | tf_op jit(solution)/shard_map/ppermute | solution.py:78
  14.2 3.6 %collective-permute-start.5 = (bf16[64,256]{1,0:T(8,128)(2,1)S(1)}, bf16[64,256]{1,0:T(8,128)(2,1)S(1)}, u32[]{:S(2)}, u32[]{:S(2)}) collective-permute-start(bf16[64,256]{1,0:T(8,128)(2,1)S(1)} %bitcast.111), channel_id=1, source_target_pairs={{0,3},{1,2},{2,1},{3,0},{4,7},{5,6},{6,5},{7,4},{8,11},{9,10},{10,... | collective-permute-start | bytes 98312 | tf_op jit(solution)/shard_map/ppermute | solution.py:78
  34.0 1.5 %collective-permute-start.6 = (bf16[512,256]{1,0:T(8,128)(2,1)S(1)}, bf16[512,256]{1,0:T(8,128)(2,1)S(1)}, u32[]{:S(2)}, u32[]{:S(2)}) collective-permute-start(bf16[512,256]{1,0:T(8,128)(2,1)S(1)} %bitcast.107), channel_id=1, source_target_pairs={{0,1},{1,0},{2,3},{3,2},{4,5},{5,4},{6,7},{7,6},{8,9},{9,8},{10,11... | collective-permute-start | bytes 786440 | tf_op jit(solution)/shard_map/ppermute | solution.py:103
  41.0 6.0 %copy-start.6 = (f32[64,2]{0,1:T(2,128)S(1)}, f32[64,2]{0,1:T(2,128)}, u32[]{:S(2)}) copy-start(f32[64,2]{0,1:T(2,128)} %param.33) | copy-start | bytes 1540
  41.1 1.6 %collective-permute-start.7 = (bf16[512,256]{1,0:T(8,128)(2,1)S(1)}, bf16[512,256]{1,0:T(8,128)(2,1)S(1)}, u32[]{:S(2)}, u32[]{:S(2)}) collective-permute-start(bf16[512,256]{1,0:T(8,128)(2,1)S(1)} %dynamic-slice_bitcast_fusion), channel_id=1, source_target_pairs={{0,1},{1,0},{2,3},{3,2},{4,5},{5,4},{6,7},{7,6},{8,9},{9,8},{10,11... | collective-permute-start | bytes 786440 | tf_op jit(solution)/shard_map/ppermute | solution.py:117
  43.5 13.9 %all-to-all-start.1 = ((bf16[16,32,256]{2,1,0:T(8,128)(2,1)}), bf16[16,32,256]{2,1,0:T(8,128)(2,1)S(1)}, u32[]{:S(2)}, u32[]{:S(2)}) async-start(bf16[16,32,256]{2,1,0:T(8,128)(2,1)} %bitcast.30), calls=%async_computation.1 | async-start | bytes 524288 | tf_op jit(solution)/shard_map/all_to_all | solution.py:119

commit v2 on v1

v2 whole, which is shorter than its diff:
```python
import jax
import jax.numpy as jnp
import numpy as np
from jax import lax
from jax.experimental import pallas as pl
from jax.experimental.pallas import tpu as pltpu
from jax.sharding import Mesh, PartitionSpec as P

EPS = 1e-06
LRU_SCALE = 8.0
SWAP = ((0, 1), (1, 0))
F32, BF16 = jnp.float32, jnp.bfloat16


def call(kernel, outs, *args, scratch=(), flops=0, final=(), limit=4 << 20, far=0):
    away = tuple(pltpu.with_memory_space_constraint(a, pltpu.HBM) for a in args[:far])
    near = tuple(pltpu.with_memory_space_constraint(a, pltpu.VMEM) for a in args[far:])
    return pl.pallas_call(
        kernel,
        out_shape=[
            jax.ShapeDtypeStruct(s, d) if i in final else pltpu.VMEM(s, d)
            for i, (s, d) in enumerate(outs)
        ],
        in_specs=[pl.BlockSpec(memory_space=pltpu.HBM)] * far
        + [pl.BlockSpec(memory_space=pltpu.VMEM)] * len(near),
        out_specs=[pl.BlockSpec(memory_space=pltpu.VMEM)] * len(outs),
        scratch_shapes=list(scratch),
        compiler_params=pltpu.CompilerParams(vmem_limit_bytes=limit),
        cost_estimate=pl.CostEstimate(flops=flops, bytes_accessed=0, transcendentals=0),
    )(*away, *near)


def dot(a, b):
    return jnp.dot(a, b, preferred_element_type=F32)


def tp_index():
    return lax.axis_index("xa") * lax.axis_size("xb") + lax.axis_index("xb")


def span(i, size):
    return pl.ds(pl.multiple_of(i * size, size), size)


def prepare(experts, capacity):
    def kernel(*refs):
        small, large, refs = refs[:9], refs[9:14], refs[14:]
        place, wcol, older, last_tap, gates, rate, mix_row, ffn_row = refs[:8]
        placed, held, sem, large_sem = refs[8:13], refs[13:22], refs[22], refs[23]
        copies = [pltpu.make_async_copy(a, b, sem.at[i]) for i, (a, b) in enumerate(zip(small, held))]
        more = [
            pltpu.make_async_copy(a, b, large_sem.at[i]) for i, (a, b) in enumerate(zip(large, placed))
        ]
        for c in copies + more:
            c.start()
        for c in copies:
            c.wait()
        ids, weight, conv, taps, wr, wi, lam, mix_gain, ffn_gain = held
        top, seqs = ids.shape
        earlier = (
            lax.broadcasted_iota(jnp.int32, (seqs, seqs), 0)
            < lax.broadcasted_iota(jnp.int32, (seqs, seqs), 1)
        ).astype(BF16)
        same = lax.broadcasted_iota(jnp.int32, (seqs, seqs), 0) == lax.broadcasted_iota(
            jnp.int32, (seqs, seqs), 1
        )
        number = lax.broadcasted_iota(jnp.int32, (experts, seqs), 0)
        base = jnp.zeros((experts, 1), F32)
        for k in range(top):
            row = ids[k : k + 1, :]
            named = (number == row).astype(F32)
            before = dot(named.astype(BF16), earlier) + base
            slot = jnp.sum(before * named, axis=0, keepdims=True)
            place[k : k + 1, :] = row * capacity + slot.astype(jnp.int32)
            base = base + jnp.sum(named, axis=1, keepdims=True)
            column = jnp.sum(jnp.where(same, weight[k : k + 1, :], 0.0), axis=1, keepdims=True)
            wcol[k] = jnp.broadcast_to(column, wcol.shape[1:])
        total = conv[0].astype(F32) * taps[0:1, :].astype(F32)
        for j in range(1, conv.shape[0]):
            total = total + conv[j].astype(F32) * taps[j : j + 1, :].astype(F32)
        older[...] = total
        last_tap[...] = taps[conv.shape[0] :, :].astype(F32)
        heads, width = wr.shape[0], wr.shape[1]
        gates[...] = jnp.zeros_like(gates)
        for h in range(heads):
            at = slice(h * width, (h + 1) * width)
            gates[at, at] = wr[h]
            gates[at, heads * width + h * width : heads * width + (h + 1) * width] = wi[h]
        rate[...] = -LRU_SCALE * jnp.log1p(jnp.exp(-lam[...])).reshape(rate.shape)
        mix_row[...] = mix_gain[...].astype(F32).reshape(mix_row.shape)
        ffn_row[...] = ffn_gain[...].astype(F32).reshape(ffn_row.shape)
        for c in more:
            c.wait()

    return kernel


def load(*refs):
    *refs, done, sem = refs
    n = len(refs) // 2
    done[...] = jnp.zeros_like(done)
    copies = [pltpu.make_async_copy(refs[i], refs[n + 1 + i], sem.at[i]) for i in range(n)]
    for c in copies:
        c.start()
    for c in copies:
        c.wait()


def mixer(t0, t1, t2, t3, mix_row, w_branch, w_gate, older, last_tap, gates, rate, state, w_out, state_out, p0, p1, p2, p3):
    me = tp_index()
    quarter = t0.shape[1]
    pieces = [t[...].astype(F32) for t in (t0, t1, t2, t3)]
    squares = sum(jnp.sum(p * p, axis=1, keepdims=True) for p in pieces)
    scale = lax.rsqrt(squares / (len(pieces) * quarter) + EPS)
    branch = gate_in = 0.0
    for k, p in enumerate(pieces):
        at = span(me ^ k, quarter)
        normed = (p * scale * mix_row[:, at]).astype(BF16)
        branch = branch + dot(normed, w_branch[at, :])
        gate_in = gate_in + dot(normed, w_gate[at, :])
    branch = branch.astype(BF16).astype(F32)
    gate_in = gate_in.astype(BF16).astype(F32)
    conv_out = older[...] + branch * last_tap[...]
    both = dot(conv_out.astype(BF16), gates[...])
    channels = conv_out.shape[1]
    recur = jax.nn.sigmoid(both[:, :channels])
    inject = jax.nn.sigmoid(both[:, channels:])
    log_decay = recur * rate[...]
    y = -2.0 * log_decay
    series = y * (1.0 - y * (1 / 2) * (1.0 - y * (1 / 3) * (1.0 - y * (1 / 4) * (1.0 - y * (1 / 5)))))
    left = jnp.where(y < 0.1, series, 1.0 - jnp.exp(-y))
    out = jnp.exp(log_decay) * state[...] + jnp.sqrt(left) * inject * conv_out
    state_out[...] = out
    lru_out = (out * jax.nn.gelu(gate_in)).astype(BF16)
    for k, p in enumerate((p0, p1, p2, p3)):
        p[...] = dot(lru_out, w_out[:, span(me ^ k, quarter)]).astype(BF16)


def hits_of(place, k, slots):
    return lax.broadcasted_iota(jnp.int32, (slots, place.shape[1]), 0) == place[k : k + 1, :]


def send_rows(tokens, p0, p1, p2, p3, place, loaded, resid, sent):
    mix_out = sum(p[...].astype(F32) for p in (p0, p1, p2, p3)).astype(BF16).astype(F32)
    rows = (tokens[...].astype(F32) + mix_out).astype(BF16)
    resid[...] = rows
    copies = lax.axis_size("xa")
    slots = sent.shape[0] // copies
    named = sum(hits_of(place, k, slots).astype(F32) for k in range(place.shape[0])).astype(BF16)
    buffer = dot(named, rows).astype(BF16)
    for a in range(copies):
        sent[a * slots : (a + 1) * slots, :] = buffer


def experts_of(mine, theirs, ffn_row, w_gate, w_up, w_down, keep, give, rows):
    b = lax.axis_index("xb")
    na, nb = lax.axis_size("xa"), lax.axis_size("xb")
    slots, quarter = mine.shape[0] // na, mine.shape[1]
    squares = 0.0
    for a in range(na):
        for part in (mine, theirs):
            v = part[a * slots : (a + 1) * slots, :].astype(F32)
            squares = squares + jnp.sum(v * v, axis=1, keepdims=True)
    scale = lax.rsqrt(squares / rows.shape[1] + EPS)
    for a in range(na):
        for part, c in ((mine, b), (theirs, 1 - b)):
            at = span(a * nb + c, quarter)
            v = part[a * slots : (a + 1) * slots, :].astype(F32)
            rows[:, at] = (v * scale * ffn_row[:, at]).astype(BF16)
    first = dot(rows[...], w_gate[0])
    second = dot(rows[...], w_up[0])
    hidden = (jax.nn.silu(first) * second).astype(BF16)
    for a in range(na):
        for part, c in ((give, 1 - b), (keep, b)):
            at = span(a * nb + c, quarter)
            part[a * slots : (a + 1) * slots, :] = dot(hidden, w_down[0, :, at]).astype(BF16)


def add_pair(keep, other, out):
    out[...] = (keep[...].astype(F32) + other[...].astype(F32)).astype(BF16)


def combine(resid, back, place, wcol, mixed):
    slots = back.shape[0] // lax.axis_size("xa")
    width = wcol.shape[2]
    total = [resid[:, i : i + width].astype(F32) for i in range(0, resid.shape[1], width)]
    for k in range(place.shape[0]):
        named = hits_of(place, k, slots).astype(F32).astype(BF16)
        picked = sum(
            lax.dot_general(
                named, back[a : a + slots, :], (((0,), (0,)), ((), ())), preferred_element_type=F32
            )
            for a in range(0, back.shape[0], slots)
        )
        for i in range(len(total)):
            total[i] = total[i] + picked[:, i * width : (i + 1) * width] * wcol[k]
    for i, v in enumerate(total):
        mixed[:, i * width : (i + 1) * width] = v.astype(BF16)


def body(
    tokens,
    conv_state,
    lru_state,
    mix_gain,
    ffn_gain,
    w_branch,
    w_gate,
    conv_taps,
    w_recur,
    w_inject,
    lru_lambda,
    w_out,
    expert_gate,
    expert_up,
    expert_down,
    route_ids,
    route_weight,
):
    seqs, quarter = tokens.shape
    top = route_ids.shape[1]
    channels = lru_state.shape[1]
    tp = ("xa", "xb")
    na = lax.axis_size("xa")
    n_tp = na * lax.axis_size("xb")
    features = n_tp * quarter
    experts = lax.axis_size("ep") * expert_gate.shape[0]
    capacity = max(2, 2 * seqs * top // experts)
    slots = experts * capacity

    def swapped(x, k):
        return lax.ppermute(x, tp, [(i, i ^ k) for i in range(n_tp)])

    others = [swapped(tokens, k) for k in range(1, n_tp)]
    small = (
        route_ids.T,
        route_weight.T,
        conv_state.transpose(1, 0, 2),
        conv_taps,
        w_recur,
        w_inject,
        lru_lambda,
        mix_gain,
        ffn_gain,
    )
    large = (tokens, lru_state, w_branch, w_gate, w_out)
    place, wcol, older, last_tap, gates, rate, mix_row, ffn_row, here, state, w_b, w_g, w_o = call(
        prepare(experts, capacity),
        [
            ((top, seqs), jnp.int32),
            ((top, seqs, 128), F32),
            ((seqs, channels), F32),
            ((1, channels), F32),
            ((channels, 2 * channels), BF16),
            ((1, channels), F32),
            ((1, features), F32),
            ((1, features), F32),
        ]
        + [(a.shape, a.dtype) for a in large],
        *small,
        *large,
        far=len(small) + len(large),
        scratch=[pltpu.VMEM(a.shape, a.dtype) for a in small]
        + [pltpu.SemaphoreType.DMA((len(small),)), pltpu.SemaphoreType.DMA((len(large),))],
        flops=10**6,
    )
    state_out, *parts = call(
        mixer,
        [((seqs, channels), F32)] + [((seqs, quarter), BF16)] * n_tp,
        here,
        *others,
        mix_row,
        w_b,
        w_g,
        older,
        last_tap,
        gates,
        rate,
        state,
        w_o,
        flops=10**8,
        final=(0,),
    )
    weights = (expert_gate, expert_up, expert_down)
    w_eg, w_eu, w_ed, loaded = call(
        load,
        [(a.shape, a.dtype) for a in weights] + [((8, 128), F32)],
        *weights,
        parts[0],
        far=len(weights),
        scratch=[pltpu.SemaphoreType.DMA((len(weights),))],
        flops=10**6,
    )
    got = [parts[0]] + [swapped(parts[k], k) for k in range(1, n_tp)]
    resid, sent = call(
        send_rows,
        [((seqs, quarter), BF16), ((na * slots, quarter), BF16)],
        here,
        *got,
        place,
        loaded,
        flops=10**7,
    )
    mine = lax.all_to_all(sent, ("xa", "ep"), split_axis=0, concat_axis=0, tiled=True)
    theirs = lax.ppermute(mine, "xb", SWAP)
    keep, give = call(
        experts_of,
        [((na * slots, quarter), BF16)] * 2,
        mine,
        theirs,
        ffn_row,
        w_eg,
        w_eu,
        w_ed,
        scratch=[pltpu.VMEM((slots, features), BF16)],
        flops=10**9,
        limit=10 << 20,
    )
    (pair,) = call(add_pair, [((na * slots, quarter), BF16)], keep, lax.ppermute(give, "xb", SWAP))
    back = lax.all_to_all(pair, ("xa", "ep"), split_axis=0, concat_axis=0, tiled=True)
    (mixed,) = call(combine, [((seqs, quarter), BF16)], resid, back, place, wcol, final=(0,))
    return (mixed, state_out)


def solution(mesh):
    n_ep, n_tp = mesh.shape["ep"], mesh.shape["tp"]
    finer = Mesh(np.asarray(mesh.devices).reshape(n_ep, n_tp // 2, 2), ("ep", "xa", "xb"))
    tp = ("xa", "xb")
    placed = (
        P("ep", tp),
        P("ep", None, tp),
        P("ep", tp),
        P(),
        P(),
        P(None, tp),
        P(None, tp),
        P(None, tp),
        P(tp, None, None),
        P(tp, None, None),
        P(tp),
        P(tp, None),
        P("ep", None, tp),
        P("ep", None, tp),
        P("ep", tp, None),
        P("ep", None),
        P("ep", None),
    )
    return jax.shard_map(
        body, mesh=finer, in_specs=placed, out_specs=(P("ep", tp), P("ep", tp)), check_vma=False
    )
```

time: 59.2 us -> 49.2 us (0.83)
  blocking collectives: 16 us -> 30 us
  waiting for transfers between devices: 16.7 us -> 5.75 us
  matrix products: 7.68 us -> 0 us
  Pallas kernels: 0 us -> 7.34 us
  other arithmetic: 5.54 us -> 0 us
  starting transfers between devices: 9.06 us -> 5.25 us
  local copies, waits for them, and re-layouts: 2.7 us -> 0 us
    all_to_all x0 -> x1, blocking collectives: none -> 13.3 us  [body(): lax.all_to_all(pair, ('xa', 'ep'), split_axis=0, concat_axis=0, tiled=True)]
    all_to_all x1 -> x0, waiting for transfers between devices: 10.3 us -> none  [body(): lax.all_to_all(pair, ('xa', 'ep'), split_axis=0, concat_axis=0, tiled=True)]
    dot_general x11 -> x0, matrix products: 7.68 us -> none  [the longest x1 2.44 us: body(): jnp.dot(hidden, expert_down[0], preferred_element_type=jnp.float32)]
    pallas_call x0 -> x7, Pallas kernels: none -> 7.34 us  [call(): pl.pallas_call(kernel, out_shape=[jax.ShapeDtypeStruct(s, d) if i in fina...]
    all_to_all x1 -> x0, starting transfers between devices: 3.53 us -> none  [body(): lax.all_to_all(pair, ('xa', 'ep'), split_axis=0, concat_axis=0, tiled=True)]
    convert_element_type x7 -> x0, other arithmetic: 2.44 us -> none  [the longest x2 0.88 us: rms_rows(): return (scaled * gain.astype(jnp.float32)).astype(jnp.bfloat16)]
    another operation x2 -> x0, other arithmetic: 0.95 us -> none  [the longest x1 0.78 us: body(): pieces = jnp.stack([tokens] + others)]
    unnamed x26 -> x0, local copies, waits for them, and re-layouts: 0.85 us -> none
  transfers between devices with their start and end apart: 9 -> 8, of which waited for: 5 -> 5; matrix products, arithmetic and copies ran while one was open for 8% -> 0% of each run, Pallas kernels for 0% -> 7%
where the time goes in v2:
time: 49.2 us; the launch traced here: 49 us
  blocking collectives  30 us (61%)
  Pallas kernels  7.34 us (15%)
  waiting for transfers between devices  5.75 us (12%)
  starting transfers between devices  5.25 us (11%)
  between operations  0.69 us (1%)
    all_to_all x1, blocking collectives, body(): lax.all_to_all(sent, ('xa', 'ep'), split_axis=0, concat_axis=0, tiled=True)  16.6 us
    all_to_all x1, blocking collectives, body(): lax.all_to_all(pair, ('xa', 'ep'), split_axis=0, concat_axis=0, tiled=True)  13.3 us
    pallas_call x7, Pallas kernels, call(): pl.pallas_call(kernel, out_shape=[jax.ShapeDtypeStruct(s, d) if i in fina...  7.34 us
    ppermute x6, starting transfers between devices, swapped(): return lax.ppermute(x, tp, [(i, i ^ k) for i in range(n_tp)])  5.05 us
    ppermute x6, waiting for transfers between devices, swapped(): return lax.ppermute(x, tp, [(i, i ^ k) for i in range(n_tp)])  2.82 us
    ppermute x1, waiting for transfers between devices, body(): theirs = lax.ppermute(mine, 'xb', SWAP)  1.53 us
    ppermute x1, waiting for transfers between devices, body(): lax.ppermute(give, 'xb', SWAP)  1.4 us
  transfers between devices with their start and end apart: 8, of which 5 were waited for; matrix products, arithmetic and copies ran while one was open for 0% of the time, Pallas kernels for 7%

profile of v2, /device:TPU:0, one launch (start us, length us, event | category | flops | bytes accessed | tf_op | source)
XLA Modules:
  0.0 49.0 jit_solution(4465083183937554118)
XLA Ops:
  0.6 0.6 %collective-permute-start = (bf16[64,256]{1,0:T(8,128)(2,1)}, bf16[64,256]{1,0:T(8,128)(2,1)S(1)}, u32[]{:S(2)}, u32[]{:S(2)}) collective-permute-start(bf16[64,256]{1,0:T(8,128)(2,1)} %refs_9_.1), channel_id=1, source_target_pairs={{0,1},{1,0},{2,3},{3,2},{4,5},{5,4},{6,7},{7,6},{8,9},{9,8},{10,11... | collective-permute-start | bytes 98312 | tf_op jit(solution)/shard_map/ppermute | solution.py:232
  1.2 2.6 %collective-permute-start.2 = (bf16[64,256]{1,0:T(8,128)(2,1)}, bf16[64,256]{1,0:T(8,128)(2,1)S(1)}, u32[]{:S(2)}, u32[]{:S(2)}) collective-permute-start(bf16[64,256]{1,0:T(8,128)(2,1)} %refs_9_.1), channel_id=1, source_target_pairs={{0,3},{1,2},{2,1},{3,0},{4,7},{5,6},{6,5},{7,4},{8,11},{9,10},{10,... | collective-permute-start | bytes 98312 | tf_op jit(solution)/shard_map/ppermute | solution.py:232
  3.8 0.0 collective-permute-start.1
  3.8 1.4 %shard_map.176 = (s32[2,64]{1,0:T(2,128)S(1)}, f32[2,64,128]{2,1,0:T(8,128)S(1)}, f32[64,128]{1,0:T(8,128)S(1)}, f32[1,128]{1,0:T(1,128)S(1)}, bf16[128,256]{1,0...) custom-call(s32[2,64]{1,0:T(2,128)} %bitcast.13, ...), custom_call_target="tpu_custom_call" | custom-call | flops 1000000 | tf_op jit(solution)/shard_map/pallas_call | solution.py:18
  5.2 0.0 collective-permute-done.t1
  5.2 0.5 collective-permute-done.2.t3
  5.7 2.2 %collective-permute-done.1.t2 = bf16[64,256]{1,0:T(8,128)(2,1)S(1)} collective-permute-done((bf16[64,256]{1,0:T(8,128)(2,1)}, bf16[64,256]{1,0:T(8,128)(2,1)S(1)}, u32[]{:S(2)}, u32[]{:S(2)}) %collective-permute-start.1) | collective-permute-done | bytes 32800 | tf_op jit(solution)/shard_map/ppermute | solution.py:232
  7.9 1.1 %shard_map.177 = (f32[64,128]{1,0:T(8,128)}, bf16[64,256]{1,0:T(8,128)(2,1)S(1)}, bf16[64,256]{1,0:T(8,128)(2,1)S(1)}, bf16[64,256]{1,0:T(8,128)(2,1)S(1)}, bf16[64,256]{1,0:T(8,128)(2,1)S(1)}) custom-call(bf16[64,256]{1,0:T(8,128)(2,1)S(1)} %get-tuple-element.28.t0.tokens, bf16[64,256]{1,0:T(8,128)(2,1)S(1)} %collective-permute-done.t1, ...), custom_call_target="tpu_custom_call" | custom-call | flops 100000000 | tf_op jit(solution)/shard_map/pallas_call | solution.py:18
  9.0 0.0 collective-permute-start.3
  9.0 0.4 collective-permute-start.4
  9.5 1.4 %collective-permute-start.5 = (bf16[64,256]{1,0:T(8,128)(2,1)S(1)}, bf16[64,256]{1,0:T(8,128)(2,1)S(1)}, u32[]{:S(2)}, u32[]{:S(2)}) collective-permute-start(bf16[64,256]{1,0:T(8,128)(2,1)S(1)} %get-tuple-element.41), channel_id=1, source_target_pairs={{0,3},{1,2},{2,1},{3,0},{4,7},{5,6},{6,5},{7,4},{8,11},{9,10},{10,... | collective-permute-start | bytes 98312 | tf_op jit(solution)/shard_map/ppermute | solution.py:232
  10.9 2.1 %shard_map.178 = (bf16[1,1024,640]{2,1,0:T(8,128)(2,1)S(1)}, bf16[1,1024,640]{2,1,0:T(8,128)(2,1)S(1)}, bf16[1,640,1024]{2,1,0:T(8,128)(2,1)S(1)}, f32[8,128]{1,0:T(8,128)S(1)}) custom-call(bf16[1,1024,640]{2,1,0:T(8,128)(2,1)} %refs_0_.1, bf16[1,1024,640]{2,1,0:T(8,128)(2,1)} %refs_1_.1, bf16[1,640,1024]{2,1,0:T(8,128)(2,1)} %refs_2_.1, ...), custom_call_target="tpu_custom_call" | custom-call | flops 1000000 | tf_op jit(solution)/shard_map/pallas_call | solution.py:18
  13.0 0.0 collective-permute-done.3.p1
  13.0 0.1 collective-permute-done.4.p2
  13.2 0.0 collective-permute-done.5.p3
  13.2 0.2 shard_map.179
  13.4 16.6 %all_to_all.22 = bf16[16,32,256]{2,1,0:T(8,128)(2,1)S(1)} all-to-all(bf16[16,32,256]{2,1,0:T(8,128)(2,1)S(1)} %bitcast.11), channel_id=1, replica_groups=mesh['ep'=8,'xa'=2,'xb'=2] {'xa','ep'}, dimensions={0} | all-to-all | bytes 524288 | tf_op jit(solution)/shard_map/all_to_all | solution.py:304
  30.0 0.0 collective-permute-start.6
  30.0 1.5 %collective-permute-done.6.theirs = bf16[512,256]{1,0:T(8,128)(2,1)S(1)} collective-permute-done((bf16[512,256]{1,0:T(8,128)(2,1)S(1)}, bf16[512,256]{1,0:T(8,128)(2,1)S(1)}, u32[]{:S(2)}, u32[]{:S(2)}) %collective-permute-start.6) | collective-permute-done | bytes 262176 | tf_op jit(solution)/shard_map/ppermute | solution.py:305
  31.6 1.6 %shard_map.180 = (bf16[512,256]{1,0:T(8,128)(2,1)S(1)}, bf16[512,256]{1,0:T(8,128)(2,1)S(1)}) custom-call(bf16[512,256]{1,0:T(8,128)(2,1)S(1)} %bitcast.8, bf16[512,256]{1,0:T(8,128)(2,1)S(1)} %collective-permute-done.6.theirs, f32[1,1024]{1,0:T(1,128)S(1)} %get-tuple-element.46.ffn_row, bf16[1,1024,640]{2,1,0:T(8,128)(2,1)S(1)} %get-tuple-element.47.w_gate, ...), custom_call_target="tpu_custom_call" | custom-call | flops 1000000000 | tf_op jit(solution)/shard_map/pallas_call | solution.py:18
  33.2 0.2 collective-permute-start.7
  33.4 1.4 %collective-permute-done.7.other = bf16[512,256]{1,0:T(8,128)(2,1)S(1)} collective-permute-done((bf16[512,256]{1,0:T(8,128)(2,1)S(1)}, bf16[512,256]{1,0:T(8,128)(2,1)S(1)}, u32[]{:S(2)}, u32[]{:S(2)}) %collective-permute-start.7) | collective-permute-done | bytes 262176 | tf_op jit(solution)/shard_map/ppermute | solution.py:319
  34.8 0.1 shard_map.181
  34.8 13.3 %all_to_all.23 = bf16[16,32,256]{2,1,0:T(8,128)(2,1)S(1)} all-to-all(bf16[16,32,256]{2,1,0:T(8,128)(2,1)S(1)} %bitcast.9), channel_id=1, replica_groups=mesh['ep'=8,'xa'=2,'xb'=2] {'xa','ep'}, dimensions={0} | all-to-all | bytes 524288 | tf_op jit(solution)/shard_map/all_to_all | solution.py:320
  48.2 0.9 %shard_map.182 = bf16[64,256]{1,0:T(8,128)(2,1)} custom-call(bf16[64,256]{1,0:T(8,128)(2,1)S(1)} %get-tuple-element.44.resid, bf16[512,256]{1,0:T(8,128)(2,1)S(1)} %bitcast.10, s32[2,64]{1,0:T(2,128)S(1)} %get-tuple-element.42.place, f32[2,64,128]{2,1,0:T(8,128)S(1)} %get-tuple-element.52.wcol), custom_call_target="tpu_custom_call" | custom-call | tf_op jit(solution)/shard_map/pallas_call | solution.py:18
Async XLA Ops:
  0.6 4.6 %collective-permute-start = (bf16[64,256]{1,0:T(8,128)(2,1)}, bf16[64,256]{1,0:T(8,128)(2,1)S(1)}, u32[]{:S(2)}, u32[]{:S(2)}) collective-permute-start(bf16[64,256]{1,0:T(8,128)(2,1)} %refs_9_.1), channel_id=1, source_target_pairs={{0,1},{1,0},{2,3},{3,2},{4,5},{5,4},{6,7},{7,6},{8,9},{9,8},{10,11... | collective-permute-start | bytes 98312 | tf_op jit(solution)/shard_map/ppermute | solution.py:232
  1.2 4.5 %collective-permute-start.2 = (bf16[64,256]{1,0:T(8,128)(2,1)}, bf16[64,256]{1,0:T(8,128)(2,1)S(1)}, u32[]{:S(2)}, u32[]{:S(2)}) collective-permute-start(bf16[64,256]{1,0:T(8,128)(2,1)} %refs_9_.1), channel_id=1, source_target_pairs={{0,3},{1,2},{2,1},{3,0},{4,7},{5,6},{6,5},{7,4},{8,11},{9,10},{10,... | collective-permute-start | bytes 98312 | tf_op jit(solution)/shard_map/ppermute | solution.py:232
  3.8 4.1 %collective-permute-start.1 = (bf16[64,256]{1,0:T(8,128)(2,1)}, bf16[64,256]{1,0:T(8,128)(2,1)S(1)}, u32[]{:S(2)}, u32[]{:S(2)}) collective-permute-start(bf16[64,256]{1,0:T(8,128)(2,1)} %refs_9_.1), channel_id=1, source_target_pairs={{0,2},{1,3},{2,0},{3,1},{4,6},{5,7},{6,4},{7,5},{8,10},{9,11},{10,... | collective-permute-start | bytes 98312 | tf_op jit(solution)/shard_map/ppermute | solution.py:232
  9.0 4.0 %collective-permute-start.3 = (bf16[64,256]{1,0:T(8,128)(2,1)S(1)}, bf16[64,256]{1,0:T(8,128)(2,1)S(1)}, u32[]{:S(2)}, u32[]{:S(2)}) collective-permute-start(bf16[64,256]{1,0:T(8,128)(2,1)S(1)} %get-tuple-element.39), channel_id=1, source_target_pairs={{0,1},{1,0},{2,3},{3,2},{4,5},{5,4},{6,7},{7,6},{8,9},{9,8},{10,11... | collective-permute-start | bytes 98312 | tf_op jit(solution)/shard_map/ppermute | solution.py:232
  9.0 4.2 %collective-permute-start.4 = (bf16[64,256]{1,0:T(8,128)(2,1)S(1)}, bf16[64,256]{1,0:T(8,128)(2,1)S(1)}, u32[]{:S(2)}, u32[]{:S(2)}) collective-permute-start(bf16[64,256]{1,0:T(8,128)(2,1)S(1)} %get-tuple-element.40), channel_id=1, source_target_pairs={{0,2},{1,3},{2,0},{3,1},{4,6},{5,7},{6,4},{7,5},{8,10},{9,11},{10,... | collective-permute-start | bytes 98312 | tf_op jit(solution)/shard_map/ppermute | solution.py:232
  9.5 3.7 %collective-permute-start.5 = (bf16[64,256]{1,0:T(8,128)(2,1)S(1)}, bf16[64,256]{1,0:T(8,128)(2,1)S(1)}, u32[]{:S(2)}, u32[]{:S(2)}) collective-permute-start(bf16[64,256]{1,0:T(8,128)(2,1)S(1)} %get-tuple-element.41), channel_id=1, source_target_pairs={{0,3},{1,2},{2,1},{3,0},{4,7},{5,6},{6,5},{7,4},{8,11},{9,10},{10,... | collective-permute-start | bytes 98312 | tf_op jit(solution)/shard_map/ppermute | solution.py:232
  30.0 1.5 %collective-permute-start.6 = (bf16[512,256]{1,0:T(8,128)(2,1)S(1)}, bf16[512,256]{1,0:T(8,128)(2,1)S(1)}, u32[]{:S(2)}, u32[]{:S(2)}) collective-permute-start(bf16[512,256]{1,0:T(8,128)(2,1)S(1)} %bitcast.7), channel_id=1, source_target_pairs={{0,1},{1,0},{2,3},{3,2},{4,5},{5,4},{6,7},{7,6},{8,9},{9,8},{10,11... | collective-permute-start | bytes 786440 | tf_op jit(solution)/shard_map/ppermute | solution.py:305
  33.2 1.6 %collective-permute-start.7 = (bf16[512,256]{1,0:T(8,128)(2,1)S(1)}, bf16[512,256]{1,0:T(8,128)(2,1)S(1)}, u32[]{:S(2)}, u32[]{:S(2)}) collective-permute-start(bf16[512,256]{1,0:T(8,128)(2,1)S(1)} %get-tuple-element.51), channel_id=1, source_target_pairs={{0,1},{1,0},{2,3},{3,2},{4,5},{5,4},{6,7},{7,6},{8,9},{9,8},{10,11... | collective-permute-start | bytes 786440 | tf_op jit(solution)/shard_map/ppermute | solution.py:319

commit v3 on v2

--- a/solution.py
+++ b/solution.py
@@ -43,10 +43,10 @@
 
 
 def prepare(experts, capacity):
-    def kernel(*refs):
-        small, large, refs = refs[:9], refs[9:14], refs[14:]
+    def prepare_kernel(*refs):
+        small, large, refs = refs[:9], refs[9:15], refs[15:]
         place, wcol, older, last_tap, gates, rate, mix_row, ffn_row = refs[:8]
-        placed, held, sem, large_sem = refs[8:13], refs[13:22], refs[22], refs[23]
+        placed, held, sem, large_sem = refs[8:14], refs[14:23], refs[23], refs[24]
         copies = [pltpu.make_async_copy(a, b, sem.at[i]) for i, (a, b) in enumerate(zip(small, held))]
         more = [
             pltpu.make_async_copy(a, b, large_sem.at[i]) for i, (a, b) in enumerate(zip(large, placed))
@@ -92,7 +92,7 @@
         for c in more:
             c.wait()
 
-    return kernel
+    return prepare_kernel
 
 
 def load(*refs):
@@ -152,28 +152,49 @@
         sent[a * slots : (a + 1) * slots, :] = buffer
 
 
-def experts_of(mine, theirs, ffn_row, w_gate, w_up, w_down, keep, give, rows):
+def own_half(mine, ffn_row, w_gate, w_up, first, second, squares):
     b = lax.axis_index("xb")
     na, nb = lax.axis_size("xa"), lax.axis_size("xb")
     slots, quarter = mine.shape[0] // na, mine.shape[1]
-    squares = 0.0
+    f = s = total = 0.0
     for a in range(na):
-        for part in (mine, theirs):
-            v = part[a * slots : (a + 1) * slots, :].astype(F32)
-            squares = squares + jnp.sum(v * v, axis=1, keepdims=True)
-    scale = lax.rsqrt(squares / rows.shape[1] + EPS)
+        at = span(a * nb + b, quarter)
+        v = mine[a * slots : (a + 1) * slots, :].astype(F32)
+        total = total + jnp.sum(v * v, axis=1, keepdims=True)
+        u = (v * ffn_row[:, at]).astype(BF16)
+        f = f + dot(u, w_gate[0, at, :])
+        s = s + dot(u, w_up[0, at, :])
+    first[...] = f
+    second[...] = s
+    squares[...] = jnp.broadcast_to(total, squares.shape)
+
+
+def other_half(theirs, ffn_row, w_gate, w_up, w_down, first, second, squares, hidden, give):
+    b = 1 - lax.axis_index("xb")
+    na, nb = lax.axis_size("xa"), lax.axis_size("xb")
+    slots, quarter = theirs.shape[0] // na, theirs.shape[1]
+    f, s, total = first[...], second[...], squares[:, :1]
     for a in range(na):
-        for part, c in ((mine, b), (theirs, 1 - b)):
-            at = span(a * nb + c, quarter)
-            v = part[a * slots : (a + 1) * slots, :].astype(F32)
-            rows[:, at] = (v * scale * ffn_row[:, at]).astype(BF16)
-    first = dot(rows[...], w_gate[0])
-    second = dot(rows[...], w_up[0])
-    hidden = (jax.nn.silu(first) * second).astype(BF16)
+        at = span(a * nb + b, quarter)
+        v = theirs[a * slots : (a + 1) * slots, :].astype(F32)
+        total = total + jnp.sum(v * v, axis=1, keepdims=True)
+        u = (v * ffn_row[:, at]).astype(BF16)
+        f = f + dot(u, w_gate[0, at, :])
+        s = s + dot(u, w_up[0, at, :])
+    scale = lax.rsqrt(total / (na * nb * quarter) + EPS)
+    h = (jax.nn.silu(f * scale) * (s * scale)).astype(BF16)
+    hidden[...] = h
     for a in range(na):
-        for part, c in ((give, 1 - b), (keep, b)):
-            at = span(a * nb + c, quarter)
-            part[a * slots : (a + 1) * slots, :] = dot(hidden, w_down[0, :, at]).astype(BF16)
+        give[a * slots : (a + 1) * slots, :] = dot(h, w_down[0, :, span(a * nb + b, quarter)]).astype(BF16)
+
+
+def kept_half(hidden, w_down, keep):
+    b = lax.axis_index("xb")
+    na, nb = lax.axis_size("xa"), lax.axis_size("xb")
+    slots, quarter = hidden.shape[0], keep.shape[1]
+    for a in range(na):
+        at = span(a * nb + b, quarter)
+        keep[a * slots : (a + 1) * slots, :] = dot(hidden[...], w_down[0, :, at]).astype(BF16)
 
 
 def add_pair(keep, other, out):
@@ -198,7 +219,7 @@
         mixed[:, i * width : (i + 1) * width] = v.astype(BF16)
 
 
-def body(
+def step(
     tokens,
     conv_state,
     lru_state,
@@ -243,8 +264,8 @@
         mix_gain,
         ffn_gain,
     )
-    large = (tokens, lru_state, w_branch, w_gate, w_out)
-    place, wcol, older, last_tap, gates, rate, mix_row, ffn_row, here, state, w_b, w_g, w_o = call(
+    large = (tokens, lru_state, w_branch, w_gate, w_out, expert_down)
+    place, wcol, older, last_tap, gates, rate, mix_row, ffn_row, here, state, w_b, w_g, w_o, w_ed = call(
         prepare(experts, capacity),
         [
             ((top, seqs), jnp.int32),
@@ -281,8 +302,8 @@
         flops=10**8,
         final=(0,),
     )
-    weights = (expert_gate, expert_up, expert_down)
-    w_eg, w_eu, w_ed, loaded = call(
+    weights = (expert_gate, expert_up)
+    w_eg, w_eu, loaded = call(
         load,
         [(a.shape, a.dtype) for a in weights] + [((8, 128), F32)],
         *weights,
@@ -303,20 +324,34 @@
     )
     mine = lax.all_to_all(sent, ("xa", "ep"), split_axis=0, concat_axis=0, tiled=True)
     theirs = lax.ppermute(mine, "xb", SWAP)
-    keep, give = call(
-        experts_of,
-        [((na * slots, quarter), BF16)] * 2,
+    ff = expert_gate.shape[2]
+    first, second, squares = call(
+        own_half,
+        [((slots, ff), F32), ((slots, ff), F32), ((slots, 128), F32)],
         mine,
+        ffn_row,
+        w_eg,
+        w_eu,
+        flops=10**8,
+        limit=8 << 20,
+    )
+    hidden, give = call(
+        other_half,
+        [((slots, ff), BF16), ((na * slots, quarter), BF16)],
         theirs,
         ffn_row,
         w_eg,
         w_eu,
         w_ed,
-        scratch=[pltpu.VMEM((slots, features), BF16)],
-        flops=10**9,
-        limit=10 << 20,
-    )
-    (pair,) = call(add_pair, [((na * slots, quarter), BF16)], keep, lax.ppermute(give, "xb", SWAP))
+        first,
+        second,
+        squares,
+        flops=10**8,
+        limit=8 << 20,
+    )
+    other = lax.ppermute(give, "xb", SWAP)
+    (keep,) = call(kept_half, [((na * slots, quarter), BF16)], hidden, w_ed, flops=10**8)
+    (pair,) = call(add_pair, [((na * slots, quarter), BF16)], keep, other)
     back = lax.all_to_all(pair, ("xa", "ep"), split_axis=0, concat_axis=0, tiled=True)
     (mixed,) = call(combine, [((seqs, quarter), BF16)], resid, back, place, wcol, final=(0,))
     return (mixed, state_out)
@@ -345,6 +380,4 @@
         P("ep", None),
         P("ep", None),
     )
-    return jax.shard_map(
-        body, mesh=finer, in_specs=placed, out_specs=(P("ep", tp), P("ep", tp)), check_vma=False
-    )
+    return jax.shard_map(step, mesh=finer, in_specs=placed, out_specs=(P("ep", tp), P("ep", tp)), check_vma=False)

time: 49.2 us -> 48.7 us (0.990)
  waiting for transfers between devices: 5.75 us -> 4.71 us
    ppermute x2, waiting for transfers between devices: 2.93 us -> 1.93 us  [the longest x1 0.99 us: step(): other = lax.ppermute(give, 'xb', SWAP)]
    pallas_call x7 -> x9, Pallas kernels: 7.34 us -> 7.73 us  [call(): pl.pallas_call(kernel, out_shape=[jax.ShapeDtypeStruct(s, d) if i in fina...]
  transfers between devices with their start and end apart: 8 -> 8, of which waited for: 5 -> 4; matrix products, arithmetic and copies ran while one was open for 0% -> 0% of each run, Pallas kernels for 7% -> 9%
where the time goes in v3:
time: 48.7 us; the launch traced here: 48.4 us
  blocking collectives  30 us (62%)
  Pallas kernels  7.73 us (16%)
  starting transfers between devices  5.27 us (11%)
  waiting for transfers between devices  4.71 us (10%)
  between operations  0.71 us (1%)
    all_to_all x1, blocking collectives, step(): lax.all_to_all(sent, ('xa', 'ep'), split_axis=0, concat_axis=0, tiled=True)  16.6 us
    all_to_all x1, blocking collectives, step(): lax.all_to_all(pair, ('xa', 'ep'), split_axis=0, concat_axis=0, tiled=True)  13.4 us
    pallas_call x9, Pallas kernels, call(): pl.pallas_call(kernel, out_shape=[jax.ShapeDtypeStruct(s, d) if i in fina...  7.73 us
    ppermute x6, starting transfers between devices, swapped(): return lax.ppermute(x, tp, [(i, i ^ k) for i in range(n_tp)])  5.05 us
    ppermute x6, waiting for transfers between devices, swapped(): return lax.ppermute(x, tp, [(i, i ^ k) for i in range(n_tp)])  2.77 us
    ppermute x1, waiting for transfers between devices, step(): other = lax.ppermute(give, 'xb', SWAP)  0.99 us
  transfers between devices with their start and end apart: 8, of which 4 were waited for; matrix products, arithmetic and copies ran while one was open for 0% of the time, Pallas kernels for 9%

profile of v3, /device:TPU:0, one launch (start us, length us, event | category | flops | bytes accessed | tf_op | source)
XLA Modules:
  0.0 48.4 jit_solution(2269067773499339313)
XLA Ops:
  0.6 0.6 %collective-permute-start = (bf16[64,256]{1,0:T(8,128)(2,1)}, bf16[64,256]{1,0:T(8,128)(2,1)S(1)}, u32[]{:S(2)}, u32[]{:S(2)}) collective-permute-start(bf16[64,256]{1,0:T(8,128)(2,1)} %refs_9_.1), channel_id=1, source_target_pairs={{0,1},{1,0},{2,3},{3,2},{4,5},{5,4},{6,7},{7,6},{8,9},{9,8},{10,11... | collective-permute-start | bytes 98312 | tf_op jit(solution)/shard_map/ppermute | solution.py:253
  1.2 2.6 %collective-permute-start.2 = (bf16[64,256]{1,0:T(8,128)(2,1)}, bf16[64,256]{1,0:T(8,128)(2,1)S(1)}, u32[]{:S(2)}, u32[]{:S(2)}) collective-permute-start(bf16[64,256]{1,0:T(8,128)(2,1)} %refs_9_.1), channel_id=1, source_target_pairs={{0,3},{1,2},{2,1},{3,0},{4,7},{5,6},{6,5},{7,4},{8,11},{9,10},{10,... | collective-permute-start | bytes 98312 | tf_op jit(solution)/shard_map/ppermute | solution.py:253
  3.8 0.0 collective-permute-start.1
  3.8 1.8 %shard_map.176 = (s32[2,64]{1,0:T(2,128)S(1)}, f32[2,64,128]{2,1,0:T(8,128)S(1)}, f32[64,128]{1,0:T(8,128)S(1)}, f32[1,128]{1,0:T(1,128)S(1)}, bf16[128,256]{1,0...) custom-call(s32[2,64]{1,0:T(2,128)} %bitcast.13, ...), custom_call_target="tpu_custom_call" | custom-call | flops 1000000 | tf_op jit(solution)/shard_map/pallas_call | solution.py:18
  5.7 0.0 collective-permute-done.t1
  5.7 0.0 collective-permute-done.2.t3
  5.7 2.2 %collective-permute-done.1.t2 = bf16[64,256]{1,0:T(8,128)(2,1)S(1)} collective-permute-done((bf16[64,256]{1,0:T(8,128)(2,1)}, bf16[64,256]{1,0:T(8,128)(2,1)S(1)}, u32[]{:S(2)}, u32[]{:S(2)}) %collective-permute-start.1) | collective-permute-done | bytes 32800 | tf_op jit(solution)/shard_map/ppermute | solution.py:253
  7.9 1.1 %shard_map.177 = (f32[64,128]{1,0:T(8,128)}, bf16[64,256]{1,0:T(8,128)(2,1)S(1)}, bf16[64,256]{1,0:T(8,128)(2,1)S(1)}, bf16[64,256]{1,0:T(8,128)(2,1)S(1)}, bf16[64,256]{1,0:T(8,128)(2,1)S(1)}) custom-call(bf16[64,256]{1,0:T(8,128)(2,1)S(1)} %get-tuple-element.31.t0.tokens, bf16[64,256]{1,0:T(8,128)(2,1)S(1)} %collective-permute-done.t1, ...), custom_call_target="tpu_custom_call" | custom-call | flops 100000000 | tf_op jit(solution)/shard_map/pallas_call | solution.py:18
  9.0 0.0 collective-permute-start.3
  9.0 0.4 collective-permute-start.4
  9.5 1.4 %collective-permute-start.5 = (bf16[64,256]{1,0:T(8,128)(2,1)S(1)}, bf16[64,256]{1,0:T(8,128)(2,1)S(1)}, u32[]{:S(2)}, u32[]{:S(2)}) collective-permute-start(bf16[64,256]{1,0:T(8,128)(2,1)S(1)} %get-tuple-element.44), channel_id=1, source_target_pairs={{0,3},{1,2},{2,1},{3,0},{4,7},{5,6},{6,5},{7,4},{8,11},{9,10},{10,... | collective-permute-start | bytes 98312 | tf_op jit(solution)/shard_map/ppermute | solution.py:253
  10.9 1.7 %shard_map.178 = (bf16[1,1024,640]{2,1,0:T(8,128)(2,1)S(1)}, bf16[1,1024,640]{2,1,0:T(8,128)(2,1)S(1)}, f32[8,128]{1,0:T(8,128)S(1)}) custom-call(bf16[1,1024,640]{2,1,0:T(8,128)(2,1)} %refs_0_.1, bf16[1,1024,640]{2,1,0:T(8,128)(2,1)} %refs_1_.1, bf16[64,256]{1,0:T(8,128)(2,1)S(1)} %get-tuple-element.41.refs_2_.p0), custom_call_target="tpu_custom_call" | custom-call | flops 1000000 | tf_op jit(solution)/shard_map/pallas_call | solution.py:18
  12.6 0.0 collective-permute-done.3.p1
  12.6 0.5 %collective-permute-done.4.p2 = bf16[64,256]{1,0:T(8,128)(2,1)S(1)} collective-permute-done((bf16[64,256]{1,0:T(8,128)(2,1)S(1)}, bf16[64,256]{1,0:T(8,128)(2,1)S(1)}, u32[]{:S(2)}, u32[]{:S(2)}) %collective-permute-start.4) | collective-permute-done | bytes 32800 | tf_op jit(solution)/shard_map/ppermute | solution.py:253
  13.2 0.0 collective-permute-done.5.p3
  13.2 0.2 shard_map.179
  13.4 16.6 %all_to_all.22 = bf16[16,32,256]{2,1,0:T(8,128)(2,1)S(1)} all-to-all(bf16[16,32,256]{2,1,0:T(8,128)(2,1)S(1)} %bitcast.11), channel_id=1, replica_groups=mesh['ep'=8,'xa'=2,'xb'=2] {'xa','ep'}, dimensions={0} | all-to-all | bytes 524288 | tf_op jit(solution)/shard_map/all_to_all | solution.py:325
  30.0 0.0 collective-permute-start.6
  30.0 0.6 %shard_map.180 = (f32[256,640]{1,0:T(8,128)S(1)}, f32[256,640]{1,0:T(8,128)S(1)}, f32[256,128]{1,0:T(8,128)S(1)}) custom-call(bf16[512,256]{1,0:T(8,128)(2,1)S(1)} %bitcast.10, f32[1,1024]{1,0:T(1,128)S(1)} %get-tuple-element.49.ffn_row, bf16[1,1024,640]{2,1,0:T(8,128)(2,1)S(1)} %get-tuple-element.50.w_gate, bf16[1,1024,640]{2,1,0:T(8,128)(2,1)S(1)} %get-tuple-element.51.w_up), custom_call_target="tpu_custom_call" | custom-call | flops 100000000 | tf_op jit(solution)/shard_map/pallas_call | solution.py:18
  30.6 0.9 %collective-permute-done.6.theirs = bf16[512,256]{1,0:T(8,128)(2,1)S(1)} collective-permute-done((bf16[512,256]{1,0:T(8,128)(2,1)S(1)}, bf16[512,256]{1,0:T(8,128)(2,1)S(1)}, u32[]{:S(2)}, u32[]{:S(2)}) %collective-permute-start.6) | collective-permute-done | bytes 262176 | tf_op jit(solution)/shard_map/ppermute | solution.py:326
  31.6 1.0 %shard_map.181 = (bf16[256,640]{1,0:T(8,128)(2,1)S(1)}, bf16[512,256]{1,0:T(8,128)(2,1)S(1)}) custom-call(bf16[512,256]{1,0:T(8,128)(2,1)S(1)} %collective-permute-done.6.theirs, f32[1,1024]{1,0:T(1,128)S(1)} %get-tuple-element.49.ffn_row, bf16[1,1024,640]{2,1,0:T(8,128)(2,1)S(1)} %get-tuple-element.50.w_gate, ...), custom_call_target="tpu_custom_call" | custom-call | flops 100000000 | tf_op jit(solution)/shard_map/pallas_call | solution.py:18
  32.5 0.2 collective-permute-start.7
  32.8 0.4 shard_map.182.keep
  33.1 1.0 %collective-permute-done.7.other = bf16[512,256]{1,0:T(8,128)(2,1)S(1)} collective-permute-done((bf16[512,256]{1,0:T(8,128)(2,1)S(1)}, bf16[512,256]{1,0:T(8,128)(2,1)S(1)}, u32[]{:S(2)}, u32[]{:S(2)}) %collective-permute-start.7) | collective-permute-done | bytes 262176 | tf_op jit(solution)/shard_map/ppermute | solution.py:352
  34.1 0.1 shard_map.183
  34.2 13.4 %all_to_all.23 = bf16[16,32,256]{2,1,0:T(8,128)(2,1)S(1)} all-to-all(bf16[16,32,256]{2,1,0:T(8,128)(2,1)S(1)} %bitcast.7), channel_id=1, replica_groups=mesh['ep'=8,'xa'=2,'xb'=2] {'xa','ep'}, dimensions={0} | all-to-all | bytes 524288 | tf_op jit(solution)/shard_map/all_to_all | solution.py:355
  47.6 0.9 %shard_map.184 = bf16[64,256]{1,0:T(8,128)(2,1)} custom-call(bf16[64,256]{1,0:T(8,128)(2,1)S(1)} %get-tuple-element.47.resid, bf16[512,256]{1,0:T(8,128)(2,1)S(1)} %bitcast.8, s32[2,64]{1,0:T(2,128)S(1)} %get-tuple-element.45.place, f32[2,64,128]{2,1,0:T(8,128)S(1)} %get-tuple-element.58.wcol), custom_call_target="tpu_custom_call" | custom-call | tf_op jit(solution)/shard_map/pallas_call | solution.py:18
Async XLA Ops:
  0.6 5.0 %collective-permute-start = (bf16[64,256]{1,0:T(8,128)(2,1)}, bf16[64,256]{1,0:T(8,128)(2,1)S(1)}, u32[]{:S(2)}, u32[]{:S(2)}) collective-permute-start(bf16[64,256]{1,0:T(8,128)(2,1)} %refs_9_.1), channel_id=1, source_target_pairs={{0,1},{1,0},{2,3},{3,2},{4,5},{5,4},{6,7},{7,6},{8,9},{9,8},{10,11... | collective-permute-start | bytes 98312 | tf_op jit(solution)/shard_map/ppermute | solution.py:253
  1.2 4.5 %collective-permute-start.2 = (bf16[64,256]{1,0:T(8,128)(2,1)}, bf16[64,256]{1,0:T(8,128)(2,1)S(1)}, u32[]{:S(2)}, u32[]{:S(2)}) collective-permute-start(bf16[64,256]{1,0:T(8,128)(2,1)} %refs_9_.1), channel_id=1, source_target_pairs={{0,3},{1,2},{2,1},{3,0},{4,7},{5,6},{6,5},{7,4},{8,11},{9,10},{10,... | collective-permute-start | bytes 98312 | tf_op jit(solution)/shard_map/ppermute | solution.py:253
  3.8 4.1 %collective-permute-start.1 = (bf16[64,256]{1,0:T(8,128)(2,1)}, bf16[64,256]{1,0:T(8,128)(2,1)S(1)}, u32[]{:S(2)}, u32[]{:S(2)}) collective-permute-start(bf16[64,256]{1,0:T(8,128)(2,1)} %refs_9_.1), channel_id=1, source_target_pairs={{0,2},{1,3},{2,0},{3,1},{4,6},{5,7},{6,4},{7,5},{8,10},{9,11},{10,... | collective-permute-start | bytes 98312 | tf_op jit(solution)/shard_map/ppermute | solution.py:253
  9.0 3.6 %collective-permute-start.3 = (bf16[64,256]{1,0:T(8,128)(2,1)S(1)}, bf16[64,256]{1,0:T(8,128)(2,1)S(1)}, u32[]{:S(2)}, u32[]{:S(2)}) collective-permute-start(bf16[64,256]{1,0:T(8,128)(2,1)S(1)} %get-tuple-element.42), channel_id=1, source_target_pairs={{0,1},{1,0},{2,3},{3,2},{4,5},{5,4},{6,7},{7,6},{8,9},{9,8},{10,11... | collective-permute-start | bytes 98312 | tf_op jit(solution)/shard_map/ppermute | solution.py:253
  9.0 4.2 %collective-permute-start.4 = (bf16[64,256]{1,0:T(8,128)(2,1)S(1)}, bf16[64,256]{1,0:T(8,128)(2,1)S(1)}, u32[]{:S(2)}, u32[]{:S(2)}) collective-permute-start(bf16[64,256]{1,0:T(8,128)(2,1)S(1)} %get-tuple-element.43), channel_id=1, source_target_pairs={{0,2},{1,3},{2,0},{3,1},{4,6},{5,7},{6,4},{7,5},{8,10},{9,11},{10,... | collective-permute-start | bytes 98312 | tf_op jit(solution)/shard_map/ppermute | solution.py:253
  9.5 3.7 %collective-permute-start.5 = (bf16[64,256]{1,0:T(8,128)(2,1)S(1)}, bf16[64,256]{1,0:T(8,128)(2,1)S(1)}, u32[]{:S(2)}, u32[]{:S(2)}) collective-permute-start(bf16[64,256]{1,0:T(8,128)(2,1)S(1)} %get-tuple-element.44), channel_id=1, source_target_pairs={{0,3},{1,2},{2,1},{3,0},{4,7},{5,6},{6,5},{7,4},{8,11},{9,10},{10,... | collective-permute-start | bytes 98312 | tf_op jit(solution)/shard_map/ppermute | solution.py:253
  30.0 1.5 %collective-permute-start.6 = (bf16[512,256]{1,0:T(8,128)(2,1)S(1)}, bf16[512,256]{1,0:T(8,128)(2,1)S(1)}, u32[]{:S(2)}, u32[]{:S(2)}) collective-permute-start(bf16[512,256]{1,0:T(8,128)(2,1)S(1)} %bitcast.9), channel_id=1, source_target_pairs={{0,1},{1,0},{2,3},{3,2},{4,5},{5,4},{6,7},{7,6},{8,9},{9,8},{10,11... | collective-permute-start | bytes 786440 | tf_op jit(solution)/shard_map/ppermute | solution.py:326
  32.5 1.6 %collective-permute-start.7 = (bf16[512,256]{1,0:T(8,128)(2,1)S(1)}, bf16[512,256]{1,0:T(8,128)(2,1)S(1)}, u32[]{:S(2)}, u32[]{:S(2)}) collective-permute-start(bf16[512,256]{1,0:T(8,128)(2,1)S(1)} %get-tuple-element.57), channel_id=1, source_target_pairs={{0,1},{1,0},{2,3},{3,2},{4,5},{5,4},{6,7},{7,6},{8,9},{9,8},{10,11... | collective-permute-start | bytes 786440 | tf_op jit(solution)/shard_map/ppermute | solution.py:352
